TPU v7x, 256 devices: a whole 4x4x8 slice. The times are simulated.
256 devices in a mesh: sp: 16 (over y, x), tp: 16 (over z, core).
Axes of the slice: x: 4, y: 4, z: 8, core: 2. Of those that a mesh axis runs over, the one named last changes fastest.
Arguments:
- skip_stream_entry: bfloat16 [8192, 2048], P(('sp', 'tp')), may hold values from -6 to 6
- result_switch_mapped: bfloat16 [8192, 4096], P('sp', 'tp'), may hold values from -6 to 6
- channel_feed_mapped: bfloat16 [8192, 4096], P('sp', 'tp'), may hold values from -6 to 6
- write_coefficient_mapped: bfloat16 [8192, 2048], P('sp', 'tp'), may hold values from -6 to 6
- emission_coefficient_mapped: bfloat16 [8192, 2048], P('sp', 'tp'), may hold values from -6 to 6
- channel_feed_taps: bfloat16 [5, 4096], P(None, 'tp'), may hold values from -2.5 to 2.5
- write_coefficient_taps: bfloat16 [5, 2048], P(None, 'tp'), may hold values from -2.5 to 2.5
- emission_coefficient_taps: bfloat16 [5, 2048], P(None, 'tp'), may hold values from -2.5 to 2.5
- raw_increments: bfloat16 [2, 64, 8192], P(None, 'tp', 'sp'), may hold values from -6 to 6
- channel_log_fade_speed: float32 [2, 64], P(None, 'tp'), may hold values from -20 to 0
- extra_log_fade: float32 [2, 64, 8192], P(None, 'tp', 'sp'), may hold values from -1 to 0
- cluster_scaling_factor: float32 [4096], P('tp'), may hold values from 0.1 to 1.9
- blend_result_matrix: bfloat16 [4096, 2048], P('tp'), may hold values from -0.09375 to 0.09375
- routing_scaling_factor: float32 [2048], replicated, may hold values from 0.1 to 1.9
- specialist_switch_matrix: bfloat16 [32, 2048, 4096], P('sp', None, 'tp'), may hold values from -0.125 to 0.125
- specialist_widen_matrix: bfloat16 [32, 2048, 4096], P('sp', None, 'tp'), may hold values from -0.125 to 0.125
- specialist_contract_matrix: bfloat16 [32, 4096, 2048], P('sp', 'tp'), may hold values from -0.1875 to 0.1875
- picked_specialists: int32 [8192, 2], P(('sp', 'tp')), may hold values from 0 to 31, all different within a row; in each aligned block of 32 rows (0 to 31, 32 to 63, ...) at most 3 rows name the same one
- router_affinities: float32 [8192, 2], P(('sp', 'tp')), may hold values from 0.1 to 1
Outputs:
- result: bfloat16 [8192, 2048], P(('sp', 'tp'))
Inputs may be any that keep to these rules, and one draw needn't show every extreme that they name: `picked_specialists`: each row names 2 different experts. Within the rows of one device (aligned blocks of 32 rows) no expert is named more than 3 times, a bound that some block reaches.
All inputs are finite; a program needn't handle non-finite values.
Results may differ from a plain program's by a relative error of at most 0.02.
Values may be sent and summed in bfloat16 or wider, within the bound.
A program may use at most 64 MiB of HBM per device.

v0:
```python
import math

import jax
import jax.numpy as jnp
from jax import lax
from jax.sharding import PartitionSpec as P

WIDTH = 2048
HEAD_DIM = 64
GROUPS = 16
STATE = 128
CONV_W = 5
BLOCK = 128
TOP = 2
INNER = 4096


EPSILON = 1e-06


def with_halo(block, sides, width):
    for axis, dim in sides:
        count = lax.axis_size(axis)
        forward = [(i, i + 1) for i in range(count - 1)]
        backward = [(target, source) for source, target in forward]
        low = lax.ppermute(
            lax.slice_in_dim(block, block.shape[dim] - width, None, axis=dim), axis, forward
        )
        high = lax.ppermute(lax.slice_in_dim(block, 0, width, axis=dim), axis, backward)
        block = jnp.concatenate([low, block, high], axis=dim)
    return block


def in_one_piece(arrays, axis, dim, along):
    widths = [math.prod(a.shape[along:]) for a in arrays]
    both = jnp.concatenate(
        [a.reshape(*a.shape[:along], w) for a, w in zip(arrays, widths)], axis=along
    )
    filled = lax.all_gather(both, axis, axis=dim, tiled=True)
    parts = jnp.split(filled, [sum(widths[:k]) for k in range(1, len(widths))], axis=along)
    return tuple(
        (b.reshape(*filled.shape[:along], *a.shape[along:]) for a, b in zip(arrays, parts))
    )


def split_up(shard, dim, peers):
    dims = shard.shape
    parts = shard.reshape(*dims[:dim], peers, dims[dim] // peers, *dims[dim + 1 :])
    return jnp.moveaxis(parts, dim, 0)


def summed_on_arrival(shard, axis, dim):
    parts = split_up(shard, dim, lax.axis_size(axis))
    arrived = lax.all_to_all(parts, axis, split_axis=0, concat_axis=0, tiled=True)
    return arrived.astype(jnp.float32).sum(axis=0)


def centred_conv(padded, weights, series_count):
    summed = jnp.zeros((series_count, padded.shape[1]), jnp.float32)
    for offset in range(weights.shape[0]):
        summed = summed + weights[offset].astype(jnp.float32) * padded[
            offset : offset + series_count
        ].astype(jnp.float32)
    return jax.nn.silu(summed)


def local_sweep(inputs, entry_state, readout_state, log_fade_factor, softplus_increment):
    seq_len = inputs.shape[0]
    blocks = seq_len // BLOCK
    heads_here = log_fade_factor.shape[0]
    groups_here = entry_state.shape[1] // STATE
    per_group = heads_here // groups_here
    values = inputs.reshape(blocks, BLOCK, groups_here, per_group, HEAD_DIM)
    b_blocks = entry_state.reshape(blocks, BLOCK, groups_here, STATE)
    c_blocks = readout_state.reshape(blocks, BLOCK, groups_here, STATE)
    decay_blocks = log_fade_factor.reshape(groups_here, per_group, blocks, BLOCK)
    step_blocks = softplus_increment.reshape(groups_here, per_group, blocks, BLOCK)
    cumulative = jnp.cumsum(decay_blocks, axis=-1)
    group_inner = jnp.einsum("bign,bjgn->gbij", c_blocks, b_blocks)
    spread = cumulative[..., :, None] - cumulative[..., None, :]
    lower_tri = jnp.arange(BLOCK)[:, None] >= jnp.arange(BLOCK)[None, :]
    mixing = (
        jnp.exp(jnp.where(lower_tri, spread, -jnp.inf))
        * step_blocks[..., None, :]
        * group_inner[:, None]
    )
    within = jnp.einsum("gkbij,bjgkp->bigkp", mixing, values)
    to_end = jnp.exp(cumulative[..., -1:] - cumulative) * step_blocks
    block_states = jnp.einsum("gkbj,bjgkp,bjgn->bgkpn", to_end, values, b_blocks)
    block_decay = cumulative[..., -1]

    def advance(carried, pieces):
        state_piece, decay_piece = pieces
        return (carried * jnp.exp(decay_piece)[..., None, None] + state_piece, carried)

    zero_state = jnp.zeros((groups_here, per_group, HEAD_DIM, STATE), jnp.float32)
    final_state, entering = lax.scan(
        advance, zero_state, (block_states, jnp.moveaxis(block_decay, -1, 0))
    )
    before = jnp.cumsum(block_decay, axis=-1) - block_decay
    return (
        (within, entering, cumulative, before, c_blocks),
        (jnp.sum(block_decay, axis=-1), final_state),
    )


def finish_sweep(parts, carried):
    within, entering, cumulative, before, c_blocks = parts
    entering = entering + carried[None] * jnp.exp(jnp.moveaxis(before, -1, 0))[..., None, None]
    readout = jnp.einsum("bign,bgkpn->bigkp", c_blocks, entering)
    readout = readout * jnp.exp(jnp.transpose(cumulative, (2, 3, 0, 1)))[..., None]
    combined = within + readout
    return combined.reshape(combined.shape[0] * combined.shape[1], -1)


def blend_parts_list(
    channel_feed_bordered,
    write_coefficient_bordered,
    emission_coefficient_bordered,
    channel_feed_taps,
    write_coefficient_taps,
    emission_coefficient_taps,
    raw_increments,
    channel_log_fade_speed,
    extra_log_fade,
    series_count,
):
    inputs = centred_conv(channel_feed_bordered, channel_feed_taps, series_count)
    entry_state = centred_conv(write_coefficient_bordered, write_coefficient_taps, series_count)
    readout_state = centred_conv(
        emission_coefficient_bordered, emission_coefficient_taps, series_count
    )
    softplus_increment = jax.nn.softplus(raw_increments.astype(jnp.float32))
    log_fade_factor = (
        -softplus_increment * jnp.exp(channel_log_fade_speed)[..., None] + extra_log_fade
    )
    onward_pass = local_sweep(
        inputs, entry_state, readout_state, log_fade_factor[0], softplus_increment[0]
    )
    backward_pass = local_sweep(
        jnp.flip(inputs, 0),
        jnp.flip(entry_state, 0),
        jnp.flip(readout_state, 0),
        jnp.flip(log_fade_factor[1], -1),
        jnp.flip(softplus_increment[1], -1),
    )
    return (onward_pass, backward_pass)


def gated_norm(mixed_sum, result_switch_mapped, cluster_scaling_factor):
    gated = mixed_sum * jax.nn.silu(result_switch_mapped.astype(jnp.float32))
    grouped = gated.reshape(gated.shape[0], -1, INNER // GROUPS)
    normalized = grouped * lax.rsqrt(jnp.mean(grouped * grouped, axis=-1, keepdims=True) + EPSILON)
    return (normalized.reshape(gated.shape) * cluster_scaling_factor).astype(jnp.bfloat16)


def rms_scale(stream, gain):
    values = stream.astype(jnp.float32)
    return (
        values * lax.rsqrt(jnp.mean(values * values, axis=-1, keepdims=True) + EPSILON) * gain
    ).astype(jnp.bfloat16)


def fold_summaries(gathered, position):
    fwd_totals, fwd_finals, bwd_totals, bwd_finals = gathered
    device_order = jnp.arange(fwd_totals.shape[0], dtype=jnp.int32)[:, None, None]
    earlier = device_order < position
    later_side = device_order > position
    fwd_running = jnp.cumsum(fwd_totals, axis=0)
    fwd_reach = jnp.sum(jnp.where(earlier, fwd_totals, 0.0), axis=0)
    fwd_weight = jnp.exp(jnp.where(earlier, fwd_reach - fwd_running, -jnp.inf))
    bwd_running = jnp.cumsum(bwd_totals, axis=0)
    bwd_reach = jnp.sum(jnp.where(device_order <= position, bwd_totals, 0.0), axis=0)
    bwd_weight = jnp.exp(jnp.where(later_side, bwd_running - bwd_totals - bwd_reach, -jnp.inf))
    carried_fwd = jnp.einsum("jgk,jgkpn->gkpn", fwd_weight, fwd_finals)
    carried_bwd = jnp.einsum("jgk,jgkpn->gkpn", bwd_weight, bwd_finals)
    return (carried_fwd, carried_bwd)


def per_device(
    skip_stream_entry,
    result_switch_mapped,
    channel_feed_mapped,
    write_coefficient_mapped,
    emission_coefficient_mapped,
    channel_feed_taps,
    write_coefficient_taps,
    emission_coefficient_taps,
    raw_increments,
    channel_log_fade_speed,
    extra_log_fade,
    cluster_scaling_factor,
    blend_result_matrix,
    routing_scaling_factor,
    specialist_switch_matrix,
    specialist_widen_matrix,
    specialist_contract_matrix,
    picked_specialists,
    router_affinities,
):
    series_count = channel_feed_mapped.shape[0]
    rim_width = CONV_W // 2
    sources = (channel_feed_mapped, write_coefficient_mapped, emission_coefficient_mapped)
    edges = jnp.concatenate(
        [jnp.concatenate([source[:rim_width], source[-rim_width:]], 0) for source in sources], 1
    )
    rimmed = with_halo(edges, (("sp", 0),), rim_width)
    padded_list = []
    column_start = 0
    for source in sources:
        width_here = source.shape[1]
        upper_rim = rimmed[:rim_width, column_start : column_start + width_here]
        lower_rim = rimmed[-rim_width:, column_start : column_start + width_here]
        padded_list.append(jnp.concatenate([upper_rim, source, lower_rim], 0))
        column_start = column_start + width_here
    onward_pass, backward_pass = blend_parts_list(
        padded_list[0],
        padded_list[1],
        padded_list[2],
        channel_feed_taps,
        write_coefficient_taps,
        emission_coefficient_taps,
        raw_increments,
        channel_log_fade_speed,
        extra_log_fade,
        series_count,
    )
    fwd_total, fwd_final = onward_pass[1]
    bwd_total, bwd_final = backward_pass[1]
    gathered = tuple(
        (
            part.astype(jnp.float32)
            for part in in_one_piece(
                (
                    fwd_total[None].astype(jnp.bfloat16),
                    fwd_final[None].astype(jnp.bfloat16),
                    bwd_total[None].astype(jnp.bfloat16),
                    bwd_final[None].astype(jnp.bfloat16),
                ),
                "sp",
                0,
                3,
            )
        )
    )
    carried_fwd, carried_bwd = fold_summaries(gathered, lax.axis_index("sp"))
    mixed_sum = finish_sweep(onward_pass[0], carried_fwd) + jnp.flip(
        finish_sweep(backward_pass[0], carried_bwd), 0
    )
    mixed_rows = gated_norm(mixed_sum, result_switch_mapped, cluster_scaling_factor)
    rows_here = skip_stream_entry.shape[0]
    projected = summed_on_arrival(
        jnp.dot(mixed_rows, blend_result_matrix, preferred_element_type=jnp.float32).astype(
            jnp.bfloat16
        ),
        "tp",
        0,
    )
    after_mixer = (skip_stream_entry.astype(jnp.float32) + projected).astype(jnp.bfloat16)
    normed = rms_scale(after_mixer, routing_scaling_factor)
    experts_here = specialist_switch_matrix.shape[0]
    expert_count = experts_here * lax.axis_size("sp")
    capacity = max(2, 3 * TOP * rows_here // (2 * expert_count))
    slot_total = capacity * expert_count
    flat_routes = picked_specialists.reshape(-1)
    one_hot = (flat_routes[:, None] == jnp.arange(expert_count, dtype=jnp.int32)[None, :]).astype(
        jnp.int32
    )
    earlier_count = jnp.cumsum(one_hot, axis=0) - one_hot
    slot_rank = jnp.sum(earlier_count * one_hot, axis=1)
    position = slot_rank * expert_count + flat_routes
    slot_match = (position[:, None] == jnp.arange(slot_total, dtype=jnp.int32)[None, :]).astype(
        jnp.bfloat16
    )
    buffer = jnp.einsum(
        "rks,rd->sd",
        slot_match.reshape(rows_here, TOP, slot_total),
        normed,
        preferred_element_type=jnp.float32,
    ).astype(jnp.bfloat16)
    buffer = buffer.reshape(capacity, expert_count, WIDTH)
    received = lax.all_to_all(buffer, "sp", split_axis=1, concat_axis=0, tiled=True)
    data_block = lax.all_gather(received, "tp", axis=0, tiled=True)
    gate_part = jnp.einsum(
        "red,edf->ref", data_block, specialist_switch_matrix, preferred_element_type=jnp.float32
    )
    up_part = jnp.einsum(
        "red,edf->ref", data_block, specialist_widen_matrix, preferred_element_type=jnp.float32
    )
    hidden = (jax.nn.silu(gate_part) * up_part).astype(jnp.bfloat16)
    expert_out = lax.psum_scatter(
        jnp.einsum(
            "ref,efd->red", hidden, specialist_contract_matrix, preferred_element_type=jnp.float32
        ).astype(jnp.bfloat16),
        "tp",
        scatter_dimension=0,
        tiled=True,
    )
    returned = lax.all_to_all(expert_out, "sp", split_axis=0, concat_axis=1, tiled=True)
    picked = jnp.dot(
        slot_match, returned.reshape(slot_total, WIDTH), preferred_element_type=jnp.float32
    )
    weights = router_affinities / jnp.sum(router_affinities, axis=-1, keepdims=True)
    mixture = jnp.sum(weights[..., None] * picked.reshape(rows_here, TOP, WIDTH), axis=1)
    return (after_mixer.astype(jnp.float32) + mixture).astype(jnp.bfloat16)


def solution(mesh):
    in_specs = (
        P(("sp", "tp"), None),
        P("sp", "tp"),
        P("sp", "tp"),
        P("sp", "tp"),
        P("sp", "tp"),
        P(None, "tp"),
        P(None, "tp"),
        P(None, "tp"),
        P(None, "tp", "sp"),
        P(None, "tp"),
        P(None, "tp", "sp"),
        P("tp"),
        P("tp", None),
        P(),
        P("sp", None, "tp"),
        P("sp", None, "tp"),
        P("sp", "tp", None),
        P(("sp", "tp"), None),
        P(("sp", "tp"), None),
    )
    out_specs = P(("sp", "tp"), None)
    return jax.shard_map(
        per_device, mesh=mesh, in_specs=in_specs, out_specs=out_specs, check_vma=False
    )
```

profile of v0, /device:TPU:1, one launch (start us, length us, event | category | flops | bytes accessed | tf_op | source)
XLA Modules:
  0.0 358.2 jit_solution(9364167012711754162)
XLA Ops:
  6.5 0.9 fusion.92
  8.3 3.9 %collective-permute-start = (bf16[2,512]{0,1:T(8,128)(2,1)S(1)}, bf16[2,512]{0,1:T(8,128)(2,1)S(1)}, u32[]{:S(2)}, u32[]{:S(2)}) collective-permute-start(bf16[2,512]{0,1:T(8,128)(2,1)S(1)} %copy.244), channel_id=1, source_target_pairs={{0,16},{16,32},{32,48},{48,64},{64,80},{80,96},{96,112},{112,128},... | collective-permute-start | bytes 6152 | tf_op jit(solution)/shard_map/ppermute | solution.py:26
  12.5 1.3 collective-permute-start.1
  13.8 1.5 slice_convert_fusion.4
  17.2 1.2 reduce_window_sum.65
  19.5 1.2 reduce_window_sum.64
  22.3 1.4 bitcast_convert_fusion.4
  23.8 1.1 copy.245
  28.2 1.4 divide_multiply_fusion
  30.4 1.0 reshape.530
  32.3 1.4 fusion.94
  33.8 1.5 divide_multiply_fusion.1
  36.5 3.0 while.27
  39.6 1.3 broadcast_multiply_fusion.1
  41.1 0.9 broadcast.263.clone.1
  42.0 5.7 %while.26 = (s32[]{:T(128)}, f32[1,4,64,128]{3,2,1,0:T(8,128)S(1)}, f32[4,1,4,64,128]{4,3,2,1,0:T(8,128)}, f32[4,1,4]{2,1,0:T(1,128)}, f32[4,1,4,64,128]{4,3,2,1,0:T(8,128)S(1)}, /*index=5*/s32[]{:T(128)}, s32[]{:T(128)}) while((s32[]{:T(128)}, f32[1,4,64,128]{3,2,1,0:T(8,128)S(1)}, f32[4,1,4,64,128]{4,3,2,1,0:T(8,128)}, ...), condition=%wide.region_2.3_spmd.clone, body=%wide.region_1.2_spmd.clone.sunk | while | flops 131075 | bytes 656016 | solution.py:97
  47.7 1.6 concatenate.52
  56.2 1.8 copy.280
  59.2 0.9 bitcast_convert_fusion.9
  60.3 1.5 divide_multiply_fusion.2
  61.9 0.9 fusion.99
  62.9 0.9 fusion.100
  63.8 38.7 %all-gather.3.cloned.1.call-done = bf16[16,1,4,16386]{3,2,1,0:T(4,128)(2,1)} async-done(((bf16[1,1,4,16386]{3,2,1,0:T(4,128)(2,1)}), bf16[16,1,4,16386]{3,2,1,0:T(4,128)(2,1)}) %all-gather.3.cloned.1.call-update) | async-done | bytes 2097424 | tf_op jit(solution)/shard_map/all_gather | solution.py:39
  104.4 4.3 %fusion.90 = (bf16[16,1,4,8192]{3,2,1,0:T(4,128)(2,1)}, bf16[16,1,4,8192]{3,2,1,0:T(4,128)(2,1)}) fusion(bf16[16,1,4,16386]{3,2,1,0:T(4,128)(2,1)} %all-gather.3.cloned.1.call-done), kind=kLoop, calls=%fused_computation.194 | loop fusion | bytes 4194304 | tf_op jit(solution)/shard_map/split | solution.py:40
  108.7 2.2 reshape.537
  111.0 1.4 fusion.15
  112.3 1.3 fusion.10
  114.3 1.2 copy.269
  115.4 2.2 reshape.541
  118.3 1.2 convert_bitcast_fusion.2
  120.3 1.3 fusion.85
  122.2 1.4 exponential_bitcast_fusion.1
  125.1 1.3 fusion.11
  127.4 3.0 rev.26
  130.4 1.3 multiply_reduce_fusion
  131.8 2.1 convolution_convert_fusion
  134.0 9.2 %all-to-all-start = ((bf16[16,32,2048]{2,1,0:T(8,128)(2,1)}), bf16[16,32,2048]{2,1,0:T(8,128)(2,1)}, u32[]{:S(2)}, u32[]{:S(2)}) async-start(bf16[16,32,2048]{2,1,0:T(8,128)(2,1)} %bitcast.262), calls=%async_computation | async-start | bytes 4194304 | tf_op jit(solution)/shard_map/all_to_all | solution.py:54
  144.3 48.0 %all-to-all-done = bf16[16,32,2048]{2,1,0:T(8,128)(2,1)} async-done(((bf16[16,32,2048]{2,1,0:T(8,128)(2,1)}), bf16[16,32,2048]{2,1,0:T(8,128)(2,1)}, u32[]{:S(2)}, u32[]{:S(2)}) %all-to-all-start) | async-done | bytes 2097184 | tf_op jit(solution)/shard_map/all_to_all | solution.py:54
  192.3 2.0 convert_reduce_fusion
  195.2 15.4 %all_to_all.38 = bf16[3,32,2048]{2,0,1:T(4,128)(2,1)S(1)} all-to-all(bf16[3,32,2048]{2,0,1:T(4,128)(2,1)S(1)} %copy.283), channel_id=1, replica_groups=mesh['sp'=16,'tp'=16] {'sp'}, dimensions={1} | all-to-all | bytes 786432 | tf_op jit(solution)/shard_map/all_to_all | solution.py:282
  211.0 0.9 copy.286
  212.0 42.6 %all-gather.5.cloned.1.call-done = bf16[768,2,2048]{2,0,1:T(8,128)(2,1)} async-done(((bf16[48,2,2048]{2,0,1:T(8,128)(2,1)}), bf16[768,2,2048]{2,0,1:T(8,128)(2,1)}) %all-gather.5.cloned.1.call-update) | async-done | bytes 6291472 | tf_op jit(solution)/shard_map/all_gather | solution.py:283
  254.6 6.4 %fusion.101 = f32[2,768,256]{2,1,0:T(8,128)} fusion(bf16[768,2,2048]{2,0,1:T(8,128)(2,1)} %all-gather.5.cloned.1.call-done, bf16[2,2048,256]{2,1,0:T(8,128)(2,1)} %param.37), kind=kOutput, calls=%fused_computation.205 | convolution fusion | flops 1610612736 | bytes 9961472 | tf_op jit(solution)/shard_map/red,edf->ref/dot_general | solution.py:284
  261.0 10.1 %convert_bitcast_fusion = bf16[768,2,2048]{2,0,1:T(8,128)(2,1)} fusion(bf16[2,256,2048]{2,1,0:T(8,128)(2,1)S(1)} %copy-done, f32[2,768,256]{2,1,0:T(8,128)} %fusion.101, bf16[768,2,2048]{2,0,1:T(8,128)(2,1)} %all-gather.5.cloned.1.call-done, bf16[2,2048,256]{2,1,0:T(8,128)(2,1)} %param.38), kind=kOutput, calls=%fused_computation.10 | convolution fusion | flops 3226730496 | bytes 18350080 | tf_op jit(solution)/shard_map/ref,efd->red/dot_general | solution.py:292
  271.1 62.3 %reduce-scatter.2.cloned.1.call-done = bf16[48,2,2048]{2,0,1:T(8,128)(2,1)} async-done(((bf16[768,2,2048]{2,0,1:T(8,128)(2,1)}), bf16[48,2,2048]{2,0,1:T(8,128)(2,1)}) %reduce-scatter.2.cloned.1.call-update) | async-done | bytes 393232 | tf_op jit(solution)/shard_map/reduce_scatter | solution.py:291
  333.4 2.1 copy.287
  335.5 6.5 %all-to-all-start.2 = ((bf16[48,2,2048]{2,1,0:T(2,128)(2,1)}), bf16[48,2,2048]{2,1,0:T(2,128)(2,1)S(1)}, u32[]{:S(2)}, u32[]{:S(2)}) async-start(bf16[48,2,2048]{2,1,0:T(2,128)(2,1)} %copy.287), calls=%async_computation.3 | async-start | bytes 786432 | tf_op jit(solution)/shard_map/all_to_all | solution.py:299
  342.1 8.2 %all-to-all-done.2 = bf16[48,2,2048]{2,1,0:T(2,128)(2,1)S(1)} async-done(((bf16[48,2,2048]{2,1,0:T(2,128)(2,1)}), bf16[48,2,2048]{2,1,0:T(2,128)(2,1)S(1)}, u32[]{:S(2)}, u32[]{:S(2)}) %all-to-all-start.2) | async-done | bytes 393248 | tf_op jit(solution)/shard_map/all_to_all | solution.py:299
  (192 shorter events, 39.9 us)
Async XLA Ops:
  6.5 254.4 %copy-start = (bf16[2,256,2048]{2,1,0:T(8,128)(2,1)S(1)}, bf16[2,256,2048]{2,1,0:T(8,128)(2,1)}, u32[]{:S(2)}) copy-start(bf16[2,256,2048]{2,1,0:T(8,128)(2,1)} %param.39) | copy-start | bytes 6291460
  6.5 96.0 %all-gather.3.cloned.1.call-start = ((), (), s32[]{:S(2)}) async-start(), calls=%async_computation.4 | async-start | bytes 2245632 | tf_op jit(solution)/shard_map/all_gather | solution.py:39
  8.3 19.1 %collective-permute-start = (bf16[2,512]{0,1:T(8,128)(2,1)S(1)}, bf16[2,512]{0,1:T(8,128)(2,1)S(1)}, u32[]{:S(2)}, u32[]{:S(2)}) collective-permute-start(bf16[2,512]{0,1:T(8,128)(2,1)S(1)} %copy.244), channel_id=1, source_target_pairs={{0,16},{16,32},{32,48},{48,64},{64,80},{80,96},{96,112},{112,128},... | collective-permute-start | bytes 6152 | tf_op jit(solution)/shard_map/ppermute | solution.py:26
  12.5 15.0 %collective-permute-start.1 = (bf16[2,512]{0,1:T(8,128)(2,1)S(1)}, bf16[2,512]{0,1:T(8,128)(2,1)S(1)}, u32[]{:S(2)}, u32[]{:S(2)}) collective-permute-start(bf16[2,512]{0,1:T(8,128)(2,1)S(1)} %copy.247), channel_id=1, source_target_pairs={{16,0},{32,16},{48,32},{64,48},{80,64},{96,80},{112,96},{128,112},... | collective-permute-start | bytes 6152 | tf_op jit(solution)/shard_map/ppermute | solution.py:29
  18.5 9.0 %copy-start.18 = (f32[4,4]{1,0:T(4,128)}, f32[4,4]{1,0:T(4,128)S(1)}, u32[]{:S(2)}) copy-start(f32[4,4]{1,0:T(4,128)S(1)} %get-tuple-element.162) | copy-start | bytes 196
  19.5 5.4 %copy-start.20 = (f32[4,512]{1,0:T(4,128)}, f32[4,512]{1,0:T(4,128)S(1)}, u32[]{:S(2)}) copy-start(f32[4,512]{1,0:T(4,128)S(1)} %rev.22) | copy-start | bytes 24580
  20.9 6.6 %copy-start.19 = (f32[4,4]{1,0:T(4,128)}, f32[4,4]{1,0:T(4,128)S(1)}, u32[]{:S(2)}) copy-start(f32[4,4]{1,0:T(4,128)S(1)} %get-tuple-element.163) | copy-start | bytes 196
  27.5 0.7 copy-start.15
  31.5 4.7 %copy-start.2 = (f32[4,128,4,64]{1,0,3,2:T(4,128)}, f32[4,128,4,64]{1,0,3,2:T(4,128)S(1)}, u32[]{:S(2)}) copy-start(f32[4,128,4,64]{1,0,3,2:T(4,128)S(1)} %reshape.535) | copy-start | bytes 1572868
  35.4 0.8 copy-start.6
  39.6 2.4 copy-start.1
  42.0 18.1 %copy-start.16 = (bf16[2,128]{0,1:T(8,128)(2,1)S(1)}, bf16[2,128]{0,1:T(8,128)(2,1)}, u32[]{:S(2)}) copy-start(bf16[2,128]{0,1:T(8,128)(2,1)} %get-tuple-element.196) | copy-start | bytes 1540
  42.0 18.2 %copy-start.17 = (bf16[2,128]{0,1:T(8,128)(2,1)S(1)}, bf16[2,128]{0,1:T(8,128)(2,1)}, u32[]{:S(2)}) copy-start(bf16[2,128]{0,1:T(8,128)(2,1)} %get-tuple-element.198) | copy-start | bytes 1540
  47.7 15.2 %copy-start.7 = (bf16[512,128]{1,0:T(8,128)(2,1)S(1)}, bf16[512,128]{1,0:T(8,128)(2,1)}, u32[]{:S(2)}) copy-start(bf16[512,128]{1,0:T(8,128)(2,1)} %copy-done.6) | copy-start | bytes 393220
  61.9 46.8 %copy-start.8 = (bf16[512,128]{1,0:T(8,128)(2,1)}, bf16[512,128]{1,0:T(8,128)(2,1)S(1)}, u32[]{:S(2)}) copy-start(bf16[512,128]{1,0:T(8,128)(2,1)S(1)} %rev.25) | copy-start | bytes 393220
  108.7 5.0 %copy-start.13 = (f32[4,128,128]{2,1,0:T(8,128)S(1)}, f32[4,128,128]{2,1,0:T(8,128)}, u32[]{:S(2)}) copy-start(f32[4,128,128]{2,1,0:T(8,128)} %fusion.99) | copy-start | bytes 786436
  110.9 2.8 copy-start.4
  110.9 2.8 copy-start.22
  110.9 2.8 copy-start.25
  110.9 2.8 copy-start.27
  114.3 10.8 %copy-start.9 = (bf16[512,128]{1,0:T(8,128)(2,1)S(1)}, bf16[512,128]{1,0:T(8,128)(2,1)}, u32[]{:S(2)}) copy-start(bf16[512,128]{1,0:T(8,128)(2,1)} %copy-done.8) | copy-start | bytes 393220
  115.4 10.9 %copy-start.12 = (f32[4,128,128]{2,1,0:T(8,128)S(1)}, f32[4,128,128]{2,1,0:T(8,128)}, u32[]{:S(2)}) copy-start(f32[4,128,128]{2,1,0:T(8,128)} %fusion.100) | copy-start | bytes 786436
  118.3 8.1 %copy-start.21 = (f32[4,512]{1,0:T(4,128)S(1)}, f32[4,512]{1,0:T(4,128)}, u32[]{:S(2)}) copy-start(f32[4,512]{1,0:T(4,128)} %copy-done.20) | copy-start | bytes 24580
  124.4 2.0 copy-start.3
  124.4 2.0 copy-start.23
  124.4 2.1 copy-start.26
  127.0 3.4 copy-start.5
  127.0 3.4 copy-start.10
  127.4 4.4 %copy-start.30 = (f32[256]{0:T(256)S(1)}, f32[256]{0:T(256)}, u32[]{:S(2)}) copy-start(f32[256]{0:T(256)} %param.34) | copy-start | bytes 3076
  130.4 1.4 copy-start.11
  134.0 9.5 %copy-start.28 = (s32[32,2]{0,1:T(2,128)S(1)}, s32[32,2]{0,1:T(2,128)}, u32[]{:S(2)}) copy-start(s32[32,2]{0,1:T(2,128)} %param.40) | copy-start | bytes 772
  134.0 58.4 %all-to-all-start = ((bf16[16,32,2048]{2,1,0:T(8,128)(2,1)}), bf16[16,32,2048]{2,1,0:T(8,128)(2,1)}, u32[]{:S(2)}, u32[]{:S(2)}) async-start(bf16[16,32,2048]{2,1,0:T(8,128)(2,1)} %bitcast.262), calls=%async_computation | async-start | bytes 4194304 | tf_op jit(solution)/shard_map/all_to_all | solution.py:54
  143.2 51.2 %copy-start.14 = (bf16[32,2048]{1,0:T(8,128)(2,1)S(1)}, bf16[32,2048]{1,0:T(8,128)(2,1)}, u32[]{:S(2)}) copy-start(bf16[32,2048]{1,0:T(8,128)(2,1)} %param.23) | copy-start | bytes 393220
  143.2 51.3 %copy-start.24 = (f32[2048]{0:T(1024)S(1)}, f32[2048]{0:T(1024)}, u32[]{:S(2)}) copy-start(f32[2048]{0:T(1024)} %param.36) | copy-start | bytes 24580
  143.2 111.4 %all-gather.5.cloned.1.call-start = ((), (), s32[]{:S(2)}) async-start(), calls=%async_computation.5 | async-start | bytes 6684672 | tf_op jit(solution)/shard_map/all_gather | solution.py:283
  211.9 121.5 %reduce-scatter.2.cloned.1.call-start = ((), (), s32[]{:S(2)}) async-start(), calls=%async_computation.6 | async-start | bytes 6684672 | tf_op jit(solution)/shard_map/reduce_scatter | solution.py:291
  271.0 71.0 %copy-start.29 = (f32[32,2]{0,1:T(2,128)S(1)}, f32[32,2]{0,1:T(2,128)}, u32[]{:S(2)}) copy-start(f32[32,2]{0,1:T(2,128)} %param.41) | copy-start | bytes 772
  335.5 14.8 %all-to-all-start.2 = ((bf16[48,2,2048]{2,1,0:T(2,128)(2,1)}), bf16[48,2,2048]{2,1,0:T(2,128)(2,1)S(1)}, u32[]{:S(2)}, u32[]{:S(2)}) async-start(bf16[48,2,2048]{2,1,0:T(2,128)(2,1)} %copy.287), calls=%async_computation.3 | async-start | bytes 786432 | tf_op jit(solution)/shard_map/all_to_all | solution.py:299
Sparse Core Ops, SparseCore 0:
  49.5 52.9 all-gather.2
  212.0 42.4 all-gather.4
  271.2 62.1 reduce-scatter.1
where the time goes:
time: 363 us; the launch traced here: 358 us
  waiting for transfers between devices  200 us (55%)
  local copies, waits for them, and re-layouts  48 us (13%)
  other arithmetic  32.5 us (9%)
  matrix products  27.3 us (8%)
  starting transfers between devices  21.2 us (6%)
  blocking collectives  15.4 us (4%)
  between operations  13.8 us (4%)
    reduce_scatter x1, waiting for transfers between devices, per_device(): lax.psum_scatter(jnp.einsum('ref,efd->red', hidden, specialist_contract_m...  62.3 us
    all_to_all x1, waiting for transfers between devices, summed_on_arrival(): lax.all_to_all(parts, axis, split_axis=0, concat_axis=0, tiled=True)  48 us
    all_gather x1, waiting for transfers between devices, per_device(): data_block = lax.all_gather(received, 'tp', axis=0, tiled=True)  42.6 us
    all_gather x1, waiting for transfers between devices, in_one_piece(): filled = lax.all_gather(both, axis, axis=dim, tiled=True)  38.7 us
    all_to_all x1, blocking collectives, per_device(): lax.all_to_all(buffer, 'sp', split_axis=1, concat_axis=0, tiled=True)  15.4 us
    dot_general x1, matrix products, per_device(): jnp.einsum('ref,efd->red', hidden, specialist_contract_matrix, preferred_...  10.1 us
    all_to_all x1, starting transfers between devices, summed_on_arrival(): lax.all_to_all(parts, axis, split_axis=0, concat_axis=0, tiled=True)  9.23 us
    all_to_all x1, waiting for transfers between devices, per_device(): lax.all_to_all(expert_out, 'sp', split_axis=0, concat_axis=1, tiled=True)  8.2 us
  transfers between devices with their start and end apart: 7, of which 5 were waited for; matrix products, arithmetic and copies ran while one was open for 8% of the time, Pallas kernels for 0%

commit v1 on v0

--- a/solution.py
+++ b/solution.py
@@ -3,6 +3,8 @@
 import jax
 import jax.numpy as jnp
 from jax import lax
+from jax.experimental import pallas as pl
+from jax.experimental.pallas import tpu as pltpu
 from jax.sharding import PartitionSpec as P
 
 WIDTH = 2048
@@ -175,6 +177,378 @@
     carried_fwd = jnp.einsum("jgk,jgkpn->gkpn", fwd_weight, fwd_finals)
     carried_bwd = jnp.einsum("jgk,jgkpn->gkpn", bwd_weight, bwd_finals)
     return (carried_fwd, carried_bwd)
+
+
+MESH = pl.DeviceIdType.MESH
+F32 = jnp.float32
+BF16 = jnp.bfloat16
+HIGH = lax.Precision.HIGHEST
+NZ = 8
+NS = 16
+
+
+def wrap(value, count):
+    return lax.rem(value + count, count)
+
+
+def remote(source, target, send_sem, recv_sem, sp, tp):
+    return pltpu.make_async_remote_copy(
+        src_ref=source,
+        dst_ref=target,
+        send_sem=send_sem,
+        recv_sem=recv_sem,
+        device_id=(sp, tp),
+        device_id_type=MESH,
+    )
+
+
+def matmul(left, right):
+    return jnp.dot(left, right, preferred_element_type=F32)
+
+
+def greet(peers_tp, over_sp):
+    s, t = lax.axis_index("sp"), lax.axis_index("tp")
+    barrier = pltpu.get_barrier_semaphore()
+    for peer in peers_tp:
+        pl.semaphore_signal(barrier, inc=1, device_id=(s, peer), device_id_type=MESH)
+    count = len(peers_tp)
+    if over_sp:
+
+        def signal_peer(k, carry):
+            pl.semaphore_signal(
+                barrier, inc=1, device_id=(lax.rem(s + k, NS), t), device_id_type=MESH
+            )
+            return carry
+
+        lax.fori_loop(1, NS, signal_peer, 0)
+        count += NS - 1
+    pl.semaphore_wait(barrier, count)
+
+
+def ring_reduce(partial, landing4, landing3, send_sems, recv_sems, z, c, s):
+    up, down = 2 * wrap(z + 1, NZ) + c, 2 * wrap(z - 1, NZ) + c
+
+    def piece(chain, half, k):
+        downward = (chain == 0) == (half == 0)
+        hops = 4 if chain == 0 else 3
+        dest = wrap(z - hops + k, NZ) if downward else lax.rem(z + hops - k, NZ)
+        landing = landing4 if chain == 0 else landing3
+        sem = (0 if chain == 0 else 8) + 4 * half + k
+        copy = remote(
+            partial.at[dest, half],
+            landing.at[half, k],
+            send_sems.at[sem],
+            recv_sems.at[sem],
+            s,
+            down if downward else up,
+        )
+        return dest, landing, copy
+
+    def add(dest, half, landing, k):
+        total = partial[dest, half].astype(F32) + landing[half, k].astype(F32)
+        partial[dest, half] = total.astype(BF16)
+
+    order = ((0, 0), (0, 1), (1, 0), (1, 1))
+    sent = []
+    for k in range(5):
+        for chain, half in order:
+            hops = 4 if chain == 0 else 3
+            if k > hops:
+                continue
+            if k > 0:
+                _, landing, before = piece(chain, half, k - 1)
+                before.wait_recv()
+                if k < hops:
+                    dest, _, _ = piece(chain, half, k)
+                else:
+                    dest = z
+                add(dest, half, landing, k - 1)
+            if k < hops:
+                _, _, copy = piece(chain, half, k)
+                copy.start()
+                sent.append(copy)
+    for copy in sent:
+        copy.wait_send()
+
+
+def moe_kernel(
+    normed_ref,
+    after_ref,
+    picks_ref,
+    affinity_ref,
+    gate_hbm,
+    up_hbm,
+    down_hbm,
+    out_ref,
+    tokens,
+    weighed,
+    gate_w,
+    up_w,
+    down_w,
+    slots,
+    arrived,
+    back,
+    rows,
+    results,
+    landing4,
+    landing3,
+    contribution,
+    incoming,
+    local_sems,
+    pair_send,
+    pair_recv,
+    sp_send,
+    sp_recv,
+    gather_send,
+    gather_recv,
+    reduce_send,
+    reduce_recv,
+    back_send,
+    back_recv,
+):
+    s, t = lax.axis_index("sp"), lax.axis_index("tp")
+    z, c = t // 2, lax.rem(t, 2)
+    other = 2 * z + (1 - c)
+    up, down = 2 * wrap(z + 1, NZ) + c, 2 * wrap(z - 1, NZ) + c
+
+    loads = [
+        pltpu.make_async_copy(source.at[c], target.at[0], local_sems.at[k])
+        for k, (source, target) in enumerate(
+            ((gate_hbm, gate_w), (up_hbm, up_w), (down_hbm, down_w))
+        )
+    ]
+    for load in loads:
+        load.start()
+
+    greet((other, up, down), True)
+
+    expert_lane = lax.broadcasted_iota(jnp.int32, (32, 128), 1)
+    share = affinity_ref[...]
+    share = share / jnp.sum(share, axis=-1, keepdims=True)
+    own = jnp.where(picks_ref[:, 0:1] == expert_lane, share[:, 0:1], 0.0) + jnp.where(
+        picks_ref[:, 1:2] == expert_lane, share[:, 1:2], 0.0
+    )
+    weighed[c] = own
+    tokens[c] = normed_ref[...]
+    pair = [
+        remote(weighed.at[c], weighed.at[c], pair_send.at[0], pair_recv.at[0], s, other),
+        remote(normed_ref, tokens.at[c], pair_send.at[1], pair_recv.at[1], s, other),
+        remote(gate_hbm.at[1 - c], gate_w.at[1], pair_send.at[2], pair_recv.at[2], s, other),
+        remote(up_hbm.at[1 - c], up_w.at[1], pair_send.at[3], pair_recv.at[3], s, other),
+        remote(down_hbm.at[1 - c], down_w.at[1], pair_send.at[4], pair_recv.at[4], s, other),
+    ]
+    for copy in pair:
+        copy.start()
+    pair[0].wait_recv()
+    pair[1].wait_recv()
+
+    weight = weighed[...].reshape(64, 128)
+    named = jnp.where(weight > 0.0, 1.0, 0.0)
+    token_row = lax.broadcasted_iota(jnp.int32, (64, 64), 0)
+    token_col = lax.broadcasted_iota(jnp.int32, (64, 64), 1)
+    earlier = jnp.where(
+        (token_col < token_row) & ((token_col >= 32) == (token_row >= 32)), 1.0, 0.0
+    )
+    rank = matmul(earlier.astype(BF16), named.astype(BF16))
+    lane_e = lax.broadcasted_iota(jnp.int32, (128, 128), 0)
+    slot_lane = lax.broadcasted_iota(jnp.int32, (128, 128), 1)
+    spread = jnp.where(lane_e == 2 * (slot_lane // 8) + c, 1.0, 0.0)
+    place = lax.rem(lax.broadcasted_iota(jnp.int32, (64, 128), 1), 8)
+    second = jnp.where(place >= 3, 1, 0)
+    token_core = jnp.where(lax.broadcasted_iota(jnp.int32, (64, 128), 0) >= 32, 1, 0)
+    wanted = (place - 3 * second).astype(F32)
+    named_slot = matmul(named.astype(BF16), spread.astype(BF16))
+    rank_slot = matmul(rank.astype(BF16), spread.astype(BF16))
+    chosen = (
+        (named_slot > 0.5) & (jnp.abs(rank_slot - wanted) < 0.5) & (token_core == second)
+        & (place < 6)
+    )
+    onehot = jnp.where(chosen, 1.0, 0.0)
+    weight_slot = jnp.where(
+        chosen, jnp.dot(weight, spread, precision=HIGH, preferred_element_type=F32), 0.0
+    )
+    everything = tokens[...].reshape(64, WIDTH)
+    filled = matmul(onehot.T.astype(BF16), everything)
+    slots[...] = filled.reshape(NS, 8, WIDTH).astype(BF16)
+
+    def send_slots(k, carry):
+        peer = lax.rem(s + k, NS)
+        remote(slots.at[peer], arrived.at[s], sp_send.at[k], sp_recv.at[k], peer, t).start()
+        return carry
+
+    lax.fori_loop(1, NS, send_slots, 0)
+    arrived[s] = slots[s]
+
+    def await_slots(k, carry):
+        remote(slots.at[s], arrived.at[s], sp_send.at[k], sp_recv.at[k], s, t).wait_recv()
+        return carry
+
+    lax.fori_loop(1, NS, await_slots, 0)
+
+    dense_row = lax.broadcasted_iota(jnp.int32, (96, 128), 0)
+    padded_row = lax.broadcasted_iota(jnp.int32, (96, 128), 1)
+    dense = jnp.where(padded_row == 8 * (dense_row // 6) + lax.rem(dense_row, 6), 1.0, 0.0)
+    padded = arrived[...].astype(F32).reshape(128, WIDTH).astype(BF16)
+    packed = matmul(dense.astype(BF16), padded).astype(BF16)
+    rows[z] = packed.reshape(2, 48, WIDTH)
+
+    def hop(upward, half, k):
+        chunk = wrap(z - k, NZ) if upward else lax.rem(z + k, NZ)
+        sem = (0 if upward else 8) + 4 * half + k
+        return remote(
+            rows.at[chunk, half],
+            rows.at[chunk, half],
+            gather_send.at[sem],
+            gather_recv.at[sem],
+            s,
+            up if upward else down,
+        )
+
+    def arrival(upward, half, k):
+        chunk = wrap(z - k - 1, NZ) if upward else lax.rem(z + k + 1, NZ)
+        sem = (0 if upward else 8) + 4 * half + k
+        return remote(
+            rows.at[chunk, half],
+            rows.at[chunk, half],
+            gather_send.at[sem],
+            gather_recv.at[sem],
+            s,
+            up if upward else down,
+        )
+
+    for upward, half in ((True, 0), (False, 1), (True, 1), (False, 0)):
+        hop(upward, half, 0).start()
+    for load in loads:
+        load.wait()
+    for copy in pair[2:]:
+        copy.wait_recv()
+
+    def step(i, carry):
+        k = (i - 1) // 2
+
+        @pl.when(lax.rem(i, 2) == 1)
+        def _():
+            for upward, half in ((True, 0), (False, 1)):
+                arrival(upward, half, k).wait_recv()
+
+                @pl.when(k < 3)
+                def _():
+                    hop(upward, half, k + 1).start()
+
+            @pl.when(k < 3)
+            def _():
+                for upward, half in ((True, 1), (False, 0)):
+                    arrival(upward, half, k).wait_recv()
+
+                    @pl.when(k < 2)
+                    def _():
+                        hop(upward, half, k + 1).start()
+
+        shift = (i + 1) // 2
+        chunk = jnp.where(lax.rem(i, 2) == 1, wrap(z - shift, NZ), lax.rem(z + shift, NZ))
+        x = rows[chunk].reshape(96, WIDTH)
+        total = None
+        for part in range(2):
+            gate = matmul(x, gate_w[part])
+            wide = matmul(x, up_w[part])
+            hidden = (gate * jax.nn.sigmoid(gate) * wide).astype(BF16)
+            piece = matmul(hidden, down_w[part])
+            total = piece if total is None else total + piece
+        results[chunk] = total.astype(BF16).reshape(2, 48, WIDTH)
+        return carry
+
+    lax.fori_loop(0, 8, step, 0)
+    for upward in (True, False):
+        for half in (0, 1):
+            for k in range(4 if upward == (half == 0) else 3):
+                hop(upward, half, k).wait_send()
+
+    ring_reduce(results, landing4, landing3, reduce_send, reduce_recv, z, c, s)
+
+    def end_slots(k, carry):
+        remote(slots.at[s], arrived.at[s], sp_send.at[k], sp_recv.at[k], s, t).wait_send()
+        return carry
+
+    lax.fori_loop(1, NS, end_slots, 0)
+    for copy in pair:
+        copy.wait_send()
+
+    reduced = results[z].reshape(96, WIDTH)
+    opened = matmul(dense.T.astype(BF16), reduced)
+    slots[...] = opened.reshape(NS, 8, WIDTH).astype(BF16)
+
+    def send_back(k, carry):
+        peer = lax.rem(s + k, NS)
+        remote(slots.at[peer], back.at[s], back_send.at[k], back_recv.at[k], peer, t).start()
+        return carry
+
+    lax.fori_loop(1, NS, send_back, 0)
+    back[s] = slots[s]
+
+    def await_back(k, carry):
+        remote(slots.at[s], back.at[s], back_send.at[k], back_recv.at[k], s, t).wait_recv()
+        return carry
+
+    lax.fori_loop(1, NS, await_back, 0)
+    answers = back[...].astype(F32).reshape(128, WIDTH).astype(BF16)
+    high = weight_slot.astype(BF16)
+    low = (weight_slot - high.astype(F32)).astype(BF16)
+    mixture = matmul(high, answers) + matmul(low, answers)
+    contribution[...] = mixture.reshape(2, 32, WIDTH)
+    swap = remote(contribution.at[1 - c], incoming, pair_send.at[5], pair_recv.at[5], s, other)
+    swap.start()
+    kept = contribution[c] + after_ref[...].astype(F32)
+    swap.wait_recv()
+    out_ref[...] = (kept + incoming[...]).astype(BF16)
+    swap.wait_send()
+
+    def end_back(k, carry):
+        remote(slots.at[s], back.at[s], back_send.at[k], back_recv.at[k], s, t).wait_send()
+        return carry
+
+    lax.fori_loop(1, NS, end_back, 0)
+
+
+def moe(normed, after, picks, affinity, gate, up, down):
+    vmem = pl.BlockSpec(memory_space=pltpu.VMEM)
+    hbm = pl.BlockSpec(memory_space=pl.ANY)
+    dma = pltpu.SemaphoreType.DMA
+    return pl.pallas_call(
+        moe_kernel,
+        out_shape=jax.ShapeDtypeStruct((32, WIDTH), BF16),
+        in_specs=[vmem] * 4 + [hbm] * 3,
+        out_specs=vmem,
+        scratch_shapes=[
+            pltpu.VMEM((2, 32, WIDTH), BF16),
+            pltpu.VMEM((2, 32, 128), F32),
+            pltpu.VMEM((2, WIDTH, 256), BF16),
+            pltpu.VMEM((2, WIDTH, 256), BF16),
+            pltpu.VMEM((2, 256, WIDTH), BF16),
+            pltpu.VMEM((NS, 8, WIDTH), BF16),
+            pltpu.VMEM((NS, 8, WIDTH), BF16),
+            pltpu.VMEM((NS, 8, WIDTH), BF16),
+            pltpu.VMEM((NZ, 2, 48, WIDTH), BF16),
+            pltpu.VMEM((NZ, 2, 48, WIDTH), BF16),
+            pltpu.VMEM((2, 4, 48, WIDTH), BF16),
+            pltpu.VMEM((2, 3, 48, WIDTH), BF16),
+            pltpu.VMEM((2, 32, WIDTH), F32),
+            pltpu.VMEM((32, WIDTH), F32),
+            dma((3,)),
+            dma((6,)),
+            dma((6,)),
+            dma((NS,)),
+            dma((NS,)),
+            dma((16,)),
+            dma((16,)),
+            dma((16,)),
+            dma((16,)),
+            dma((NS,)),
+            dma((NS,)),
+        ],
+        compiler_params=pltpu.CompilerParams(
+            collective_id=0, has_side_effects=True, vmem_limit_bytes=56 * 1024 * 1024
+        ),
+    )(normed, after, picks, affinity, gate, up, down)
 
 
 def per_device(
@@ -258,51 +632,15 @@
     )
     after_mixer = (skip_stream_entry.astype(jnp.float32) + projected).astype(jnp.bfloat16)
     normed = rms_scale(after_mixer, routing_scaling_factor)
-    experts_here = specialist_switch_matrix.shape[0]
-    expert_count = experts_here * lax.axis_size("sp")
-    capacity = max(2, 3 * TOP * rows_here // (2 * expert_count))
-    slot_total = capacity * expert_count
-    flat_routes = picked_specialists.reshape(-1)
-    one_hot = (flat_routes[:, None] == jnp.arange(expert_count, dtype=jnp.int32)[None, :]).astype(
-        jnp.int32
-    )
-    earlier_count = jnp.cumsum(one_hot, axis=0) - one_hot
-    slot_rank = jnp.sum(earlier_count * one_hot, axis=1)
-    position = slot_rank * expert_count + flat_routes
-    slot_match = (position[:, None] == jnp.arange(slot_total, dtype=jnp.int32)[None, :]).astype(
-        jnp.bfloat16
-    )
-    buffer = jnp.einsum(
-        "rks,rd->sd",
-        slot_match.reshape(rows_here, TOP, slot_total),
+    return moe(
         normed,
-        preferred_element_type=jnp.float32,
-    ).astype(jnp.bfloat16)
-    buffer = buffer.reshape(capacity, expert_count, WIDTH)
-    received = lax.all_to_all(buffer, "sp", split_axis=1, concat_axis=0, tiled=True)
-    data_block = lax.all_gather(received, "tp", axis=0, tiled=True)
-    gate_part = jnp.einsum(
-        "red,edf->ref", data_block, specialist_switch_matrix, preferred_element_type=jnp.float32
-    )
-    up_part = jnp.einsum(
-        "red,edf->ref", data_block, specialist_widen_matrix, preferred_element_type=jnp.float32
-    )
-    hidden = (jax.nn.silu(gate_part) * up_part).astype(jnp.bfloat16)
-    expert_out = lax.psum_scatter(
-        jnp.einsum(
-            "ref,efd->red", hidden, specialist_contract_matrix, preferred_element_type=jnp.float32
-        ).astype(jnp.bfloat16),
-        "tp",
-        scatter_dimension=0,
-        tiled=True,
-    )
-    returned = lax.all_to_all(expert_out, "sp", split_axis=0, concat_axis=1, tiled=True)
-    picked = jnp.dot(
-        slot_match, returned.reshape(slot_total, WIDTH), preferred_element_type=jnp.float32
-    )
-    weights = router_affinities / jnp.sum(router_affinities, axis=-1, keepdims=True)
-    mixture = jnp.sum(weights[..., None] * picked.reshape(rows_here, TOP, WIDTH), axis=1)
-    return (after_mixer.astype(jnp.float32) + mixture).astype(jnp.bfloat16)
+        after_mixer,
+        picked_specialists,
+        router_affinities,
+        specialist_switch_matrix,
+        specialist_widen_matrix,
+        specialist_contract_matrix,
+    )
 
 
 def solution(mesh):

time: 363 us -> 269 us (0.74)
  waiting for transfers between devices: 200 us -> 88.6 us
  Pallas kernels: 0 us -> 91.5 us
  other arithmetic: 32.5 us -> 14.8 us
  matrix products: 27.3 us -> 10.5 us
  blocking collectives: 15.4 us -> 0 us
  local copies, waits for them, and re-layouts: 48 us -> 33.6 us
  starting transfers between devices: 21.2 us -> 14.5 us
    pallas_call x0 -> x1, Pallas kernels: none -> 91.5 us  [moe(): pl.pallas_call(moe_kernel, out_shape=jax.ShapeDtypeStruct((32, WIDTH), BF...]
    reduce_scatter x1 -> x0, waiting for transfers between devices: 62.3 us -> none  [per_device(): lax.psum_scatter(jnp.einsum('ref,efd->red', hidden, specialist_contract_m...]
    all_gather x1 -> x0, waiting for transfers between devices: 42.6 us -> none  [per_device(): data_block = lax.all_gather(received, 'tp', axis=0, tiled=True)]
    dot_general x4 -> x0, matrix products: 17.1 us -> none  [the longest x1 10.1 us: per_device(): jnp.einsum('ref,efd->red', hidden, specialist_contract_matrix, preferred_...]
    all_to_all x1 -> x0, blocking collectives: 15.4 us -> none  [per_device(): lax.all_to_all(buffer, 'sp', split_axis=1, concat_axis=0, tiled=True)]
    all_to_all x1 -> x0, waiting for transfers between devices: 8.2 us -> none  [per_device(): lax.all_to_all(expert_out, 'sp', split_axis=0, concat_axis=1, tiled=True)]
    all_to_all x1 -> x0, starting transfers between devices: 6.51 us -> none  [per_device(): lax.all_to_all(expert_out, 'sp', split_axis=0, concat_axis=1, tiled=True)]
  transfers between devices with their start and end apart: 7 -> 4, of which waited for: 5 -> 2; matrix products, arithmetic and copies ran while one was open for 8% -> 9% of each run, Pallas kernels for 0% -> 0%
where the time goes in v1:
time: 269 us; the launch traced here: 268 us
  Pallas kernels  91.5 us (34%)
  waiting for transfers between devices  88.6 us (33%)
  local copies, waits for them, and re-layouts  33.6 us (12%)
  other arithmetic  14.8 us (6%)
  starting transfers between devices  14.5 us (5%)
  between operations  14.1 us (5%)
  matrix products  10.5 us (4%)
    pallas_call x1, Pallas kernels, moe(): pl.pallas_call(moe_kernel, out_shape=jax.ShapeDtypeStruct((32, WIDTH), BF...  91.5 us
    all_to_all x1, waiting for transfers between devices, summed_on_arrival(): lax.all_to_all(parts, axis, split_axis=0, concat_axis=0, tiled=True)  47.6 us
    all_gather x1, waiting for transfers between devices, in_one_piece(): filled = lax.all_gather(both, axis, axis=dim, tiled=True)  40.9 us
    all_to_all x1, starting transfers between devices, summed_on_arrival(): lax.all_to_all(parts, axis, split_axis=0, concat_axis=0, tiled=True)  9.23 us
    unnamed x80, local copies, waits for them, and re-layouts  6.42 us
  transfers between devices with their start and end apart: 4, of which 2 were waited for; matrix products, arithmetic and copies ran while one was open for 9% of the time, Pallas kernels for 0%

profile of v1, /device:TPU:1, one launch (start us, length us, event | category | flops | bytes accessed | tf_op | source)
XLA Modules:
  0.0 267.8 jit_solution(3657924690648464174)
XLA Ops:
  6.5 0.8 fusion.76
  7.3 0.7 fusion.79
  8.3 3.9 %collective-permute-start = (bf16[2,512]{0,1:T(8,128)(2,1)S(1)}, bf16[2,512]{0,1:T(8,128)(2,1)S(1)}, u32[]{:S(2)}, u32[]{:S(2)}) collective-permute-start(bf16[2,512]{0,1:T(8,128)(2,1)S(1)} %copy.133), channel_id=1, source_target_pairs={{0,16},{16,32},{32,48},{48,64},{64,80},{80,96},{96,112},{112,128},... | collective-permute-start | bytes 6152 | tf_op jit(solution)/shard_map/ppermute | solution.py:28
  12.4 1.3 collective-permute-start.1
  13.7 0.9 slice_convert_fusion.4
  14.6 0.7 exp.107
  15.3 0.8 compare_select_fusion
  16.5 1.2 reduce_window_sum.54
  18.9 1.2 reduce_window_sum.53
  20.5 0.9 bitcast_convert_fusion.4
  21.3 1.1 copy.134
  22.5 0.7 copy.147
  23.2 0.7 copy.153
  23.9 0.7 copy.152
  24.7 0.8 divide_multiply_fusion
  25.4 0.8 rev.23
  30.2 3.0 %while.26 = (s32[]{:T(128)}, f32[1,4,64,128]{3,2,1,0:T(8,128)S(1)}, f32[4,1,4,64,128]{4,3,2,1,0:T(8,128)S(1)}, f32[4,1,4]{2,1,0:T(1,128)}, f32[4,1,4,64,128]{4,3,2,1,0:T(8,128)S(1)}, /*index=5*/s32[]{:T(128)}, s32[]{:T(128)}) while((s32[]{:T(128)}, f32[1,4,64,128]{3,2,1,0:T(8,128)S(1)}, f32[4,1,4,64,128]{4,3,2,1,0:T(8,128)S(1)}, ...), condition=%wide.region_2.3_spmd.clone, body=%wide.region_1.2_spmd.clone.sunk | while | flops 131075 | bytes 655508 | solution.py:99
  31.0 0.7 fusion.98
  31.8 0.7 fusion.98
  33.3 1.6 concatenate.52
  35.0 0.8 reduce_window_sum.57
  35.8 0.7 exponential_bitcast_fusion.5
  36.5 0.7 copy.156
  38.4 0.8 reduce_window_sum.59
  41.8 0.9 copy.169
  43.8 0.9 bitcast_convert_fusion.9
  45.3 0.9 fusion.83
  46.2 0.9 fusion.84
  47.2 40.9 %all-gather.2.cloned.1.call-done = bf16[16,1,4,16386]{3,2,1,0:T(4,128)(2,1)} async-done(((bf16[1,1,4,16386]{3,2,1,0:T(4,128)(2,1)}), bf16[16,1,4,16386]{3,2,1,0:T(4,128)(2,1)}) %all-gather.2.cloned.1.call-update) | async-done | bytes 2097424 | tf_op jit(solution)/shard_map/all_gather | solution.py:41
  88.1 0.8 fusion.75
  89.4 4.0 %fusion.74 = (bf16[16,1,4,8192]{3,2,1,0:T(4,128)(2,1)}, bf16[16,1,4,8192]{3,2,1,0:T(4,128)(2,1)S(1)}) fusion(bf16[16,1,4,16386]{3,2,1,0:T(4,128)(2,1)} %all-gather.2.cloned.1.call-done), kind=kLoop, calls=%fused_computation.166 | loop fusion | bytes 4194304 | tf_op jit(solution)/shard_map/split | solution.py:42
  93.4 2.2 reshape.483
  95.6 0.7 fusion.10
  96.3 1.3 fusion.6
  98.3 1.1 copy.158
  99.4 1.1 reshape.487
  101.1 0.7 fusion.8
  101.8 1.3 fusion.7
  103.1 1.5 fusion.4
  105.1 0.8 rev.26
  106.1 2.2 convolution_convert_fusion
  108.3 9.2 %all-to-all-start = ((bf16[16,32,2048]{2,1,0:T(8,128)(2,1)}), bf16[16,32,2048]{2,1,0:T(8,128)(2,1)S(1)}, u32[]{:S(2)}, u32[]{:S(2)}) async-start(bf16[16,32,2048]{2,1,0:T(8,128)(2,1)} %bitcast.220), calls=%async_computation | async-start | bytes 4194304 | tf_op jit(solution)/shard_map/all_to_all | solution.py:56
  117.5 0.7 copy.170.picks_ref
  118.2 0.7 copy.171.affinity_ref
  118.9 47.6 %all-to-all-done = bf16[16,32,2048]{2,1,0:T(8,128)(2,1)S(1)} async-done(((bf16[16,32,2048]{2,1,0:T(8,128)(2,1)}), bf16[16,32,2048]{2,1,0:T(8,128)(2,1)S(1)}, u32[]{:S(2)}, u32[]{:S(2)}) %all-to-all-start) | async-done | bytes 2097184 | tf_op jit(solution)/shard_map/all_to_all | solution.py:56
  167.1 0.8 fusion.52.normed_ref
  167.9 91.5 %shard_map.181 = bf16[32,2048]{1,0:T(8,128)(2,1)} custom-call(bf16[32,2048]{1,0:T(8,128)(2,1)} %fusion.52.normed_ref, bf16[32,2048]{1,0:T(8,128)(2,1)} %copy-done.8, s32[32,2]{1,0:T(8,128)} %copy.170.picks_ref, f32[32,2]{1,0:T(8,128)} %copy.171.affinity_ref, bf16[2,2048,256]{2,1,0:T(8,128)(2,1)} %gate_hbm.1, bf16[2,2048,256]{2,1,0:T(8,128)(2,1)} %up_hbm.1, ...), custom_call_target="tpu_custom_call" | custom-call | tf_op jit(solution)/shard_map/pallas_call | solution.py:516
  259.4 1.6 copy.229
  (173 shorter events, 16.8 us)
Async XLA Ops:
  6.5 99.5 %copy-start = (bf16[256,2048]{1,0:T(8,128)(2,1)S(1)}, bf16[256,2048]{1,0:T(8,128)(2,1)}, u32[]{:S(2)}) copy-start(bf16[256,2048]{1,0:T(8,128)(2,1)} %param.35) | copy-start | bytes 3145732
  6.5 81.5 %all-gather.2.cloned.1.call-start = ((), (), s32[]{:S(2)}) async-start(), calls=%async_computation.1 | async-start | bytes 2245632 | tf_op jit(solution)/shard_map/all_gather | solution.py:41
  8.3 16.3 %collective-permute-start = (bf16[2,512]{0,1:T(8,128)(2,1)S(1)}, bf16[2,512]{0,1:T(8,128)(2,1)S(1)}, u32[]{:S(2)}, u32[]{:S(2)}) collective-permute-start(bf16[2,512]{0,1:T(8,128)(2,1)S(1)} %copy.133), channel_id=1, source_target_pairs={{0,16},{16,32},{32,48},{48,64},{64,80},{80,96},{96,112},{112,128},... | collective-permute-start | bytes 6152 | tf_op jit(solution)/shard_map/ppermute | solution.py:28
  12.4 12.2 %collective-permute-start.1 = (bf16[2,512]{0,1:T(8,128)(2,1)S(1)}, bf16[2,512]{0,1:T(8,128)(2,1)S(1)}, u32[]{:S(2)}, u32[]{:S(2)}) collective-permute-start(bf16[2,512]{0,1:T(8,128)(2,1)S(1)} %copy.136), channel_id=1, source_target_pairs={{16,0},{32,16},{48,32},{64,48},{80,64},{96,80},{112,96},{128,112},... | collective-permute-start | bytes 6152 | tf_op jit(solution)/shard_map/ppermute | solution.py:31
  17.9 6.8 %copy-start.17 = (f32[4,4]{1,0:T(4,128)}, f32[4,4]{1,0:T(4,128)S(1)}, u32[]{:S(2)}) copy-start(f32[4,4]{1,0:T(4,128)S(1)} %get-tuple-element.142) | copy-start | bytes 196
  18.8 3.6 %copy-start.21 = (f32[4,512]{1,0:T(4,128)}, f32[4,512]{1,0:T(4,128)S(1)}, u32[]{:S(2)}) copy-start(f32[4,512]{1,0:T(4,128)S(1)} %rev.22) | copy-start | bytes 24580
  20.3 4.4 %copy-start.18 = (f32[4,4]{1,0:T(4,128)}, f32[4,4]{1,0:T(4,128)S(1)}, u32[]{:S(2)}) copy-start(f32[4,4]{1,0:T(4,128)S(1)} %get-tuple-element.143) | copy-start | bytes 196
  24.7 3.4 %copy-start.12 = (bf16[512,128]{1,0:T(8,128)(2,1)S(1)}, bf16[512,128]{1,0:T(8,128)(2,1)}, u32[]{:S(2)}) copy-start(bf16[512,128]{1,0:T(8,128)(2,1)} %param.26) | copy-start | bytes 393220
  26.4 3.1 %copy-start.5 = (f32[4,128,4,64]{1,0,3,2:T(4,128)}, f32[4,128,4,64]{1,0,3,2:T(4,128)S(1)}, u32[]{:S(2)}) copy-start(f32[4,128,4,64]{1,0,3,2:T(4,128)S(1)} %reshape.476) | copy-start | bytes 1572868
  26.6 2.0 copy-start.3
  29.4 0.8 copy-start.1
  29.9 11.9 %copy-start.10 = (bf16[512,256]{1,0:T(8,128)(2,1)S(1)}, bf16[512,256]{1,0:T(8,128)(2,1)}, u32[]{:S(2)}) copy-start(bf16[512,256]{1,0:T(8,128)(2,1)} %param.24) | copy-start | bytes 786436
  29.9 14.8 %copy-start.15 = (bf16[2,128]{0,1:T(8,128)(2,1)S(1)}, bf16[2,128]{0,1:T(8,128)(2,1)}, u32[]{:S(2)}) copy-start(bf16[2,128]{0,1:T(8,128)(2,1)} %get-tuple-element.176) | copy-start | bytes 1540
  29.9 14.9 %copy-start.16 = (bf16[2,128]{0,1:T(8,128)(2,1)S(1)}, bf16[2,128]{0,1:T(8,128)(2,1)}, u32[]{:S(2)}) copy-start(bf16[2,128]{0,1:T(8,128)(2,1)} %get-tuple-element.178) | copy-start | bytes 1540
  29.9 15.0 %copy-start.13 = (bf16[512,128]{1,0:T(8,128)(2,1)S(1)}, bf16[512,128]{1,0:T(8,128)(2,1)}, u32[]{:S(2)}) copy-start(bf16[512,128]{1,0:T(8,128)(2,1)} %param.27) | copy-start | bytes 393220
  33.3 60.1 %copy-start.2 = (f32[4,1,4,64,128]{4,3,2,1,0:T(8,128)}, f32[4,1,4,64,128]{4,3,2,1,0:T(8,128)S(1)}, u32[]{:S(2)}) copy-start(f32[4,1,4,64,128]{4,3,2,1,0:T(8,128)S(1)} %get-tuple-element.61) | copy-start | bytes 1572868
  93.4 2.9 %copy-start.20 = (f32[4,128,4]{1,2,0:T(4,128)S(1)}, f32[4,128,4]{1,2,0:T(4,128)}, u32[]{:S(2)}) copy-start(f32[4,128,4]{1,2,0:T(4,128)} %copy.157) | copy-start | bytes 24580
  93.4 2.9 %copy-start.25 = (f32[4,1,4]{2,0,1:T(4,128)S(1)}, f32[4,1,4]{2,0,1:T(4,128)}, u32[]{:S(2)}) copy-start(f32[4,1,4]{2,0,1:T(4,128)} %copy.156) | copy-start | bytes 196
  93.4 4.2 %copy-start.23 = (pred[128,128]{1,0:T(8,128)(4,1)S(1)}, pred[128,128]{1,0:T(8,128)(4,1)}, u32[]{:S(2)}) copy-start(pred[128,128]{1,0:T(8,128)(4,1)} %iota_compare_fusion) | copy-start | bytes 49156
  93.4 4.3 %copy-start.27 = (f32[4,4,128]{2,0,1:T(4,128)S(1)}, f32[4,4,128]{2,0,1:T(4,128)}, u32[]{:S(2)}) copy-start(f32[4,4,128]{2,0,1:T(4,128)} %get-tuple-element.183) | copy-start | bytes 24580
  93.4 4.3 %copy-start.29 = (f32[4,4,128]{2,0,1:T(4,128)S(1)}, f32[4,4,128]{2,0,1:T(4,128)}, u32[]{:S(2)}) copy-start(f32[4,4,128]{2,0,1:T(4,128)} %copy.138) | copy-start | bytes 24580
  95.6 2.1 copy-start.6
  95.6 2.1 copy-start.11
  98.3 2.5 copy-start.34
  98.3 2.7 copy-start.33
  98.3 3.5 %copy-start.19 = (f32[4,128,4]{1,2,0:T(4,128)S(1)}, f32[4,128,4]{1,2,0:T(4,128)}, u32[]{:S(2)}) copy-start(f32[4,128,4]{1,2,0:T(4,128)} %copy.167) | copy-start | bytes 24580
  98.3 3.5 %copy-start.24 = (f32[4,1,4]{2,0,1:T(4,128)S(1)}, f32[4,1,4]{2,0,1:T(4,128)}, u32[]{:S(2)}) copy-start(f32[4,1,4]{2,0,1:T(4,128)} %copy.166) | copy-start | bytes 196
  99.4 3.7 %copy-start.22 = (f32[4,512]{1,0:T(4,128)S(1)}, f32[4,512]{1,0:T(4,128)}, u32[]{:S(2)}) copy-start(f32[4,512]{1,0:T(4,128)} %copy-done.21) | copy-start | bytes 24580
  99.4 3.7 %copy-start.28 = (f32[4,4,128]{2,0,1:T(4,128)S(1)}, f32[4,4,128]{2,0,1:T(4,128)}, u32[]{:S(2)}) copy-start(f32[4,4,128]{2,0,1:T(4,128)} %copy.159) | copy-start | bytes 24580
  100.5 2.6 copy-start.4
  104.7 1.2 copy-start.7
  104.7 1.2 copy-start.9
  105.0 1.1 copy-start.32
  108.3 9.2 %copy-start.30 = (s32[32,2]{0,1:T(2,128)S(1)}, s32[32,2]{0,1:T(2,128)}, u32[]{:S(2)}) copy-start(s32[32,2]{0,1:T(2,128)} %param.40) | copy-start | bytes 772
  108.3 10.0 %copy-start.31 = (f32[32,2]{0,1:T(2,128)S(1)}, f32[32,2]{0,1:T(2,128)}, u32[]{:S(2)}) copy-start(f32[32,2]{0,1:T(2,128)} %param.41) | copy-start | bytes 772
  108.3 58.3 %all-to-all-start = ((bf16[16,32,2048]{2,1,0:T(8,128)(2,1)}), bf16[16,32,2048]{2,1,0:T(8,128)(2,1)S(1)}, u32[]{:S(2)}, u32[]{:S(2)}) async-start(bf16[16,32,2048]{2,1,0:T(8,128)(2,1)} %bitcast.220), calls=%async_computation | async-start | bytes 4194304 | tf_op jit(solution)/shard_map/all_to_all | solution.py:56
  117.5 49.4 %copy-start.14 = (bf16[32,2048]{1,0:T(8,128)(2,1)S(1)}, bf16[32,2048]{1,0:T(8,128)(2,1)}, u32[]{:S(2)}) copy-start(bf16[32,2048]{1,0:T(8,128)(2,1)} %param.23) | copy-start | bytes 393220
  117.5 49.6 %copy-start.26 = (f32[2048]{0:T(1024)S(1)}, f32[2048]{0:T(1024)}, u32[]{:S(2)}) copy-start(f32[2048]{0:T(1024)} %param.36) | copy-start | bytes 24580
  167.1 0.8 copy-start.8
Sparse Core Ops, SparseCore 0:
  35.1 52.9 all-gather.1

commit v2 on v1

--- a/solution.py
+++ b/solution.py
@@ -43,18 +43,6 @@
     return tuple(
         (b.reshape(*filled.shape[:along], *a.shape[along:]) for a, b in zip(arrays, parts))
     )
-
-
-def split_up(shard, dim, peers):
-    dims = shard.shape
-    parts = shard.reshape(*dims[:dim], peers, dims[dim] // peers, *dims[dim + 1 :])
-    return jnp.moveaxis(parts, dim, 0)
-
-
-def summed_on_arrival(shard, axis, dim):
-    parts = split_up(shard, dim, lax.axis_size(axis))
-    arrived = lax.all_to_all(parts, axis, split_axis=0, concat_axis=0, tiled=True)
-    return arrived.astype(jnp.float32).sum(axis=0)
 
 
 def centred_conv(padded, weights, series_count):
@@ -156,13 +144,6 @@
     return (normalized.reshape(gated.shape) * cluster_scaling_factor).astype(jnp.bfloat16)
 
 
-def rms_scale(stream, gain):
-    values = stream.astype(jnp.float32)
-    return (
-        values * lax.rsqrt(jnp.mean(values * values, axis=-1, keepdims=True) + EPSILON) * gain
-    ).astype(jnp.bfloat16)
-
-
 def fold_summaries(gathered, position):
     fwd_totals, fwd_finals, bwd_totals, bwd_finals = gathered
     device_order = jnp.arange(fwd_totals.shape[0], dtype=jnp.int32)[:, None, None]
@@ -228,58 +209,64 @@
 def ring_reduce(partial, landing4, landing3, send_sems, recv_sems, z, c, s):
     up, down = 2 * wrap(z + 1, NZ) + c, 2 * wrap(z - 1, NZ) + c
 
+    def dest_of(chain, half, k):
+        hops = 4 - chain
+        return wrap(z - hops + k, NZ) if chain == half else lax.rem(z + hops - k, NZ)
+
     def piece(chain, half, k):
-        downward = (chain == 0) == (half == 0)
-        hops = 4 if chain == 0 else 3
-        dest = wrap(z - hops + k, NZ) if downward else lax.rem(z + hops - k, NZ)
-        landing = landing4 if chain == 0 else landing3
-        sem = (0 if chain == 0 else 8) + 4 * half + k
-        copy = remote(
-            partial.at[dest, half],
-            landing.at[half, k],
+        sem = 8 * chain + 4 * half + k
+        return remote(
+            partial.at[dest_of(chain, half, k), half],
+            (landing3 if chain else landing4).at[half, k],
             send_sems.at[sem],
             recv_sems.at[sem],
             s,
-            down if downward else up,
+            down if chain == half else up,
         )
-        return dest, landing, copy
-
-    def add(dest, half, landing, k):
-        total = partial[dest, half].astype(F32) + landing[half, k].astype(F32)
-        partial[dest, half] = total.astype(BF16)
-
-    order = ((0, 0), (0, 1), (1, 0), (1, 1))
+
     sent = []
     for k in range(5):
-        for chain, half in order:
-            hops = 4 if chain == 0 else 3
+        for chain, half in ((0, 0), (0, 1), (1, 0), (1, 1)):
+            hops = 4 - chain
             if k > hops:
                 continue
             if k > 0:
-                _, landing, before = piece(chain, half, k - 1)
-                before.wait_recv()
-                if k < hops:
-                    dest, _, _ = piece(chain, half, k)
-                else:
-                    dest = z
-                add(dest, half, landing, k - 1)
+                piece(chain, half, k - 1).wait_recv()
             if k < hops:
-                _, _, copy = piece(chain, half, k)
+                dest = dest_of(chain, half, k)
+                if k > 0:
+                    landing = landing3 if chain else landing4
+                    total = partial[dest, half].astype(F32) + landing[half, k - 1].astype(F32)
+                    partial[dest, half] = total.astype(BF16)
+                copy = piece(chain, half, k)
                 copy.start()
                 sent.append(copy)
     for copy in sent:
         copy.wait_send()
+    return [
+        partial[z, half].astype(F32) + landing4[half, 3].astype(F32) + landing3[half, 2].astype(F32)
+        for half in (0, 1)
+    ]
 
 
 def moe_kernel(
-    normed_ref,
-    after_ref,
+    mixed_ref,
+    blend_ref,
+    skip_ref,
+    gain_ref,
     picks_ref,
     affinity_ref,
     gate_hbm,
     up_hbm,
     down_hbm,
     out_ref,
+    mixed_in,
+    blend_in,
+    projected,
+    landing4p,
+    landing3p,
+    after,
+    normed,
     tokens,
     weighed,
     gate_w,
@@ -299,6 +286,8 @@
     pair_recv,
     sp_send,
     sp_recv,
+    project_send,
+    project_recv,
     gather_send,
     gather_recv,
     reduce_send,
@@ -329,18 +318,34 @@
         picks_ref[:, 1:2] == expert_lane, share[:, 1:2], 0.0
     )
     weighed[c] = own
-    tokens[c] = normed_ref[...]
     pair = [
+        remote(mixed_ref.at[:, 1 - c], mixed_in, pair_send.at[6], pair_recv.at[6], s, other),
+        remote(blend_ref, blend_in, pair_send.at[7], pair_recv.at[7], s, other),
         remote(weighed.at[c], weighed.at[c], pair_send.at[0], pair_recv.at[0], s, other),
-        remote(normed_ref, tokens.at[c], pair_send.at[1], pair_recv.at[1], s, other),
         remote(gate_hbm.at[1 - c], gate_w.at[1], pair_send.at[2], pair_recv.at[2], s, other),
         remote(up_hbm.at[1 - c], up_w.at[1], pair_send.at[3], pair_recv.at[3], s, other),
         remote(down_hbm.at[1 - c], down_w.at[1], pair_send.at[4], pair_recv.at[4], s, other),
     ]
     for copy in pair:
         copy.start()
+
+    first = matmul(mixed_ref[:, c].reshape(256, 256), blend_ref[...])
     pair[0].wait_recv()
     pair[1].wait_recv()
+    both = first + matmul(mixed_in[...].reshape(256, 256), blend_in[...])
+    projected[...] = both.astype(BF16).reshape(NZ, 2, 16, WIDTH)
+    summed = ring_reduce(projected, landing4p, landing3p, project_send, project_recv, z, c, s)
+    stream = (skip_ref[...].astype(F32) + jnp.concatenate(summed, axis=0)).astype(BF16)
+    after[...] = stream
+    stream = stream.astype(F32)
+    scale = lax.rsqrt(jnp.mean(stream * stream, axis=-1, keepdims=True) + EPSILON)
+    normed[...] = (stream * scale * gain_ref[...]).astype(BF16)
+    tokens[c] = normed[...]
+    swap = remote(normed, tokens.at[c], pair_send.at[1], pair_recv.at[1], s, other)
+    swap.start()
+    pair[2].wait_recv()
+    swap.wait_recv()
+    pair.append(swap)
 
     weight = weighed[...].reshape(64, 128)
     named = jnp.where(weight > 0.0, 1.0, 0.0)
@@ -420,7 +425,7 @@
         hop(upward, half, 0).start()
     for load in loads:
         load.wait()
-    for copy in pair[2:]:
+    for copy in pair[3:6]:
         copy.wait_recv()
 
     def step(i, carry):
@@ -463,7 +468,7 @@
             for k in range(4 if upward == (half == 0) else 3):
                 hop(upward, half, k).wait_send()
 
-    ring_reduce(results, landing4, landing3, reduce_send, reduce_recv, z, c, s)
+    summed = ring_reduce(results, landing4, landing3, reduce_send, reduce_recv, z, c, s)
 
     def end_slots(k, carry):
         remote(slots.at[s], arrived.at[s], sp_send.at[k], sp_recv.at[k], s, t).wait_send()
@@ -473,7 +478,7 @@
     for copy in pair:
         copy.wait_send()
 
-    reduced = results[z].reshape(96, WIDTH)
+    reduced = jnp.concatenate([part.astype(BF16) for part in summed], axis=0)
     opened = matmul(dense.T.astype(BF16), reduced)
     slots[...] = opened.reshape(NS, 8, WIDTH).astype(BF16)
 
@@ -497,7 +502,7 @@
     contribution[...] = mixture.reshape(2, 32, WIDTH)
     swap = remote(contribution.at[1 - c], incoming, pair_send.at[5], pair_recv.at[5], s, other)
     swap.start()
-    kept = contribution[c] + after_ref[...].astype(F32)
+    kept = contribution[c] + after[...].astype(F32)
     swap.wait_recv()
     out_ref[...] = (kept + incoming[...]).astype(BF16)
     swap.wait_send()
@@ -509,16 +514,23 @@
     lax.fori_loop(1, NS, end_back, 0)
 
 
-def moe(normed, after, picks, affinity, gate, up, down):
+def finish_layer(mixed, blend, skip, gain, picks, affinity, gate, up, down):
     vmem = pl.BlockSpec(memory_space=pltpu.VMEM)
     hbm = pl.BlockSpec(memory_space=pl.ANY)
     dma = pltpu.SemaphoreType.DMA
     return pl.pallas_call(
         moe_kernel,
         out_shape=jax.ShapeDtypeStruct((32, WIDTH), BF16),
-        in_specs=[vmem] * 4 + [hbm] * 3,
+        in_specs=[vmem] * 6 + [hbm] * 3,
         out_specs=vmem,
         scratch_shapes=[
+            pltpu.VMEM((NZ, 32, 256), BF16),
+            pltpu.VMEM((256, WIDTH), BF16),
+            pltpu.VMEM((NZ, 2, 16, WIDTH), BF16),
+            pltpu.VMEM((2, 4, 16, WIDTH), BF16),
+            pltpu.VMEM((2, 3, 16, WIDTH), BF16),
+            pltpu.VMEM((32, WIDTH), BF16),
+            pltpu.VMEM((32, WIDTH), BF16),
             pltpu.VMEM((2, 32, WIDTH), BF16),
             pltpu.VMEM((2, 32, 128), F32),
             pltpu.VMEM((2, WIDTH, 256), BF16),
@@ -534,10 +546,12 @@
             pltpu.VMEM((2, 32, WIDTH), F32),
             pltpu.VMEM((32, WIDTH), F32),
             dma((3,)),
-            dma((6,)),
-            dma((6,)),
+            dma((8,)),
+            dma((8,)),
             dma((NS,)),
             dma((NS,)),
+            dma((16,)),
+            dma((16,)),
             dma((16,)),
             dma((16,)),
             dma((16,)),
@@ -548,7 +562,17 @@
         compiler_params=pltpu.CompilerParams(
             collective_id=0, has_side_effects=True, vmem_limit_bytes=56 * 1024 * 1024
         ),
-    )(normed, after, picks, affinity, gate, up, down)
+    )(
+        mixed.reshape(NZ, 2, 32, 256),
+        blend,
+        skip,
+        gain.reshape(1, WIDTH),
+        picks,
+        affinity,
+        gate,
+        up,
+        down,
+    )
 
 
 def per_device(
@@ -622,19 +646,11 @@
         finish_sweep(backward_pass[0], carried_bwd), 0
     )
     mixed_rows = gated_norm(mixed_sum, result_switch_mapped, cluster_scaling_factor)
-    rows_here = skip_stream_entry.shape[0]
-    projected = summed_on_arrival(
-        jnp.dot(mixed_rows, blend_result_matrix, preferred_element_type=jnp.float32).astype(
-            jnp.bfloat16
-        ),
-        "tp",
-        0,
-    )
-    after_mixer = (skip_stream_entry.astype(jnp.float32) + projected).astype(jnp.bfloat16)
-    normed = rms_scale(after_mixer, routing_scaling_factor)
-    return moe(
-        normed,
-        after_mixer,
+    return finish_layer(
+        mixed_rows,
+        blend_result_matrix,
+        skip_stream_entry,
+        routing_scaling_factor,
         picked_specialists,
         router_affinities,
         specialist_switch_matrix,

time: 269 us -> 217 us (0.81)
  waiting for transfers between devices: 88.6 us -> 47.8 us
  Pallas kernels: 91.5 us -> 112 us
  local copies, waits for them, and re-layouts: 33.6 us -> 21.4 us
  starting transfers between devices: 14.5 us -> 5.23 us
  other arithmetic: 14.8 us -> 9.7 us
  matrix products: 10.5 us -> 6.32 us
    all_to_all x1 -> x0, waiting for transfers between devices: 47.6 us -> none  [summed_on_arrival(): lax.all_to_all(parts, axis, split_axis=0, concat_axis=0, tiled=True)]
    pallas_call x1, Pallas kernels: 91.5 us -> 112 us  [finish_layer(): pl.pallas_call(moe_kernel, out_shape=jax.ShapeDtypeStruct((32, WIDTH), BF...]
    all_to_all x1 -> x0, starting transfers between devices: 9.23 us -> none  [summed_on_arrival(): lax.all_to_all(parts, axis, split_axis=0, concat_axis=0, tiled=True)]
    all_gather x1, waiting for transfers between devices: 40.9 us -> 47.7 us  [in_one_piece(): filled = lax.all_gather(both, axis, axis=dim, tiled=True)]
    unnamed x80 -> x46, local copies, waits for them, and re-layouts: 6.42 us -> 5.94 us
  transfers between devices with their start and end apart: 4 -> 3, of which waited for: 2 -> 1; matrix products, arithmetic and copies ran while one was open for 9% -> 6% of each run, Pallas kernels for 0% -> 0%
where the time goes in v2:
time: 217 us
  Pallas kernels  112 us (52%)
  waiting for transfers between devices  47.8 us (22%)
  local copies, waits for them, and re-layouts  21.4 us (10%)
  between operations  14 us (6%)
  other arithmetic  9.7 us (4%)
  matrix products  6.32 us (3%)
  starting transfers between devices  5.23 us (2%)
    pallas_call x1, Pallas kernels, finish_layer(): pl.pallas_call(moe_kernel, out_shape=jax.ShapeDtypeStruct((32, WIDTH), BF...  112 us
    all_gather x1, waiting for transfers between devices, in_one_piece(): filled = lax.all_gather(both, axis, axis=dim, tiled=True)  47.7 us
    unnamed x46, local copies, waits for them, and re-layouts  5.94 us
  transfers between devices with their start and end apart: 3, of which 1 were waited for; matrix products, arithmetic and copies ran while one was open for 6% of the time, Pallas kernels for 0%

profile of v2, /device:TPU:1, one launch (start us, length us, event | category | flops | bytes accessed | tf_op | source)
XLA Modules:
  0.0 216.9 jit_solution(12289257919009992679)
XLA Ops:
  6.5 0.7 fusion.71
  7.2 0.7 fusion.74
  8.2 3.9 %collective-permute-start = (bf16[2,512]{0,1:T(8,128)(2,1)S(1)}, bf16[2,512]{0,1:T(8,128)(2,1)S(1)}, u32[]{:S(2)}, u32[]{:S(2)}) collective-permute-start(bf16[2,512]{0,1:T(8,128)(2,1)S(1)} %copy.135), channel_id=1, source_target_pairs={{0,16},{16,32},{32,48},{48,64},{64,80},{80,96},{96,112},{112,128},... | collective-permute-start | bytes 6152 | tf_op jit(solution)/shard_map/ppermute | solution.py:28
  12.3 1.3 collective-permute-start.1
  13.6 0.9 slice_convert_fusion.4
  14.5 0.7 exp.107
  15.2 0.8 compare_select_fusion
  16.0 0.4 rev.21
  16.4 1.2 reduce_window_sum.54
  17.8 0.4 rev.22
  18.2 1.2 reduce_window_sum.53
  19.8 0.9 bitcast_convert_fusion.4
  20.7 1.1 copy.136
  22.2 0.8 divide_multiply_fusion
  23.0 0.8 rev.23
  23.7 0.2 reshape.476
  24.3 0.3 divide_multiply_fusion.1
  24.9 0.2 convolution_bitcast_fusion.3
  25.2 0.6 while.27
  26.0 0.2 convolution_bitcast_fusion.4
  26.3 0.3 copy-done
  26.6 0.6 while.26
  27.2 0.9 concatenate.52
  28.8 0.8 copy.171
  29.7 0.7 copy.173.picks_ref
  30.4 0.7 copy.174.affinity_ref
  31.3 0.3 divide_multiply_fusion.2
  31.7 0.9 fusion.78
  32.6 0.9 fusion.79
  33.5 47.7 %all-gather.2.cloned.1.call-done = bf16[16,1,4,16386]{3,2,1,0:T(4,128)(2,1)} async-done(((bf16[1,1,4,16386]{3,2,1,0:T(4,128)(2,1)}), bf16[16,1,4,16386]{3,2,1,0:T(4,128)(2,1)}) %all-gather.2.cloned.1.call-update) | async-done | bytes 2097424 | tf_op jit(solution)/shard_map/all_gather | solution.py:41
  81.3 0.8 fusion.70
  82.6 3.0 %fusion.69 = (bf16[16,1,4,8192]{3,2,1,0:T(4,128)(2,1)S(1)}, bf16[16,1,4,8192]{3,2,1,0:T(4,128)(2,1)S(1)}) fusion(bf16[16,1,4,16386]{3,2,1,0:T(4,128)(2,1)} %all-gather.2.cloned.1.call-done), kind=kLoop, calls=%fused_computation.156 | loop fusion | bytes 4194304 | tf_op jit(solution)/shard_map/split | solution.py:42
  85.6 1.1 reshape.483
  86.8 0.7 fusion.10
  87.5 1.3 fusion.6
  88.8 0.6 fusion.5
  89.4 1.1 copy.160
  90.5 1.1 reshape.487
  92.2 0.7 fusion.8
  92.8 0.3 fusion.7
  93.2 0.6 fusion.4
  93.7 0.3 copy.170
  94.1 0.8 rev.26
  94.9 0.2 multiply_reduce_fusion
  95.2 0.2 copy.172
  95.6 0.7 multiply_convert_fusion.mixed_ref
  96.3 112.1 %shard_map.181 = bf16[32,2048]{1,0:T(8,128)(2,1)} custom-call(bf16[8,2,32,256]{3,2,1,0:T(8,128)(2,1)} %multiply_convert_fusion.mixed_ref, bf16[256,2048]{1,0:T(8,128)(2,1)} %blend_ref.1, bf16[32,2048]{1,0:T(8,128)(2,1)} %skip_ref.1, f32[1,2048]{1,0:T(1,128)} %bitcast.241, s32[32,2]{1,0:T(8,128)} %copy.173.picks_ref, f32[32,2]{1,0:T(8,128)} %copy.174.affinity_ref, ...), custom_call_target="tpu_custom_call" | custom-call | tf_op jit(solution)/shard_map/pallas_call | solution.py:521
  208.4 1.6 copy.232
  (135 shorter events, 5.6 us)
Async XLA Ops:
  6.5 74.7 %all-gather.2.cloned.1.call-start = ((), (), s32[]{:S(2)}) async-start(), calls=%async_computation | async-start | bytes 2245632 | tf_op jit(solution)/shard_map/all_gather | solution.py:41
  8.2 14.0 %collective-permute-start = (bf16[2,512]{0,1:T(8,128)(2,1)S(1)}, bf16[2,512]{0,1:T(8,128)(2,1)S(1)}, u32[]{:S(2)}, u32[]{:S(2)}) collective-permute-start(bf16[2,512]{0,1:T(8,128)(2,1)S(1)} %copy.135), channel_id=1, source_target_pairs={{0,16},{16,32},{32,48},{48,64},{64,80},{80,96},{96,112},{112,128},... | collective-permute-start | bytes 6152 | tf_op jit(solution)/shard_map/ppermute | solution.py:28
  12.3 9.9 %collective-permute-start.1 = (bf16[2,512]{0,1:T(8,128)(2,1)S(1)}, bf16[2,512]{0,1:T(8,128)(2,1)S(1)}, u32[]{:S(2)}, u32[]{:S(2)}) collective-permute-start(bf16[2,512]{0,1:T(8,128)(2,1)S(1)} %copy.138), channel_id=1, source_target_pairs={{16,0},{32,16},{48,32},{64,48},{80,64},{96,80},{112,96},{128,112},... | collective-permute-start | bytes 6152 | tf_op jit(solution)/shard_map/ppermute | solution.py:31
  22.2 2.1 copy-start.12
  23.9 1.9 copy-start.5
  24.1 0.8 copy-start.3
  25.8 0.8 copy-start
  26.2 2.6 %copy-start.9 = (bf16[512,256]{1,0:T(8,128)(2,1)S(1)}, bf16[512,256]{1,0:T(8,128)(2,1)}, u32[]{:S(2)}) copy-start(bf16[512,256]{1,0:T(8,128)(2,1)} %param.24) | copy-start | bytes 786436
  26.2 3.4 %copy-start.16 = (s32[32,2]{0,1:T(2,128)S(1)}, s32[32,2]{0,1:T(2,128)}, u32[]{:S(2)}) copy-start(s32[32,2]{0,1:T(2,128)} %param.40) | copy-start | bytes 772
  26.3 4.1 %copy-start.17 = (f32[32,2]{0,1:T(2,128)S(1)}, f32[32,2]{0,1:T(2,128)}, u32[]{:S(2)}) copy-start(f32[32,2]{0,1:T(2,128)} %param.41) | copy-start | bytes 772
  26.3 4.8 %copy-start.14 = (bf16[5,128]{1,0:T(8,128)(2,1)S(1)}, bf16[5,128]{1,0:T(8,128)(2,1)}, u32[]{:S(2)}) copy-start(bf16[5,128]{1,0:T(8,128)(2,1)} %param.30) | copy-start | bytes 3844
  26.3 5.0 %copy-start.13 = (bf16[512,128]{1,0:T(8,128)(2,1)S(1)}, bf16[512,128]{1,0:T(8,128)(2,1)}, u32[]{:S(2)}) copy-start(bf16[512,128]{1,0:T(8,128)(2,1)} %param.27) | copy-start | bytes 393220
  27.2 55.4 %copy-start.2 = (f32[4,1,4,64,128]{4,3,2,1,0:T(8,128)}, f32[4,1,4,64,128]{4,3,2,1,0:T(8,128)S(1)}, u32[]{:S(2)}) copy-start(f32[4,1,4,64,128]{4,3,2,1,0:T(8,128)S(1)} %get-tuple-element.61) | copy-start | bytes 1572868
  86.8 2.0 copy-start.6
  86.8 2.0 copy-start.11
  89.4 3.5 %copy-start.1 = (f32[4,1,4,64,128]{4,3,2,1,0:T(8,128)S(1)}, f32[4,1,4,64,128]{4,3,2,1,0:T(8,128)}, u32[]{:S(2)}) copy-start(f32[4,1,4,64,128]{4,3,2,1,0:T(8,128)} %copy-done) | copy-start | bytes 1572868
  90.5 2.6 %copy-start.4 = (f32[4,128,4,64]{1,0,3,2:T(4,128)S(1)}, f32[4,128,4,64]{1,0,3,2:T(4,128)}, u32[]{:S(2)}) copy-start(f32[4,128,4,64]{1,0,3,2:T(4,128)} %copy-done.3) | copy-start | bytes 1572868
  91.6 1.5 copy-start.10
  93.2 1.7 copy-start.7
  93.2 1.7 copy-start.8
  94.9 0.7 copy-start.15
Sparse Core Ops, SparseCore 0:
  28.3 52.9 all-gather.1

commit v3 on v2

--- a/solution.py
+++ b/solution.py
@@ -1,5 +1,3 @@
-import math
-
 import jax
 import jax.numpy as jnp
 from jax import lax
@@ -9,156 +7,10 @@
 
 WIDTH = 2048
 HEAD_DIM = 64
-GROUPS = 16
 STATE = 128
 CONV_W = 5
 BLOCK = 128
-TOP = 2
-INNER = 4096
-
-
 EPSILON = 1e-06
-
-
-def with_halo(block, sides, width):
-    for axis, dim in sides:
-        count = lax.axis_size(axis)
-        forward = [(i, i + 1) for i in range(count - 1)]
-        backward = [(target, source) for source, target in forward]
-        low = lax.ppermute(
-            lax.slice_in_dim(block, block.shape[dim] - width, None, axis=dim), axis, forward
-        )
-        high = lax.ppermute(lax.slice_in_dim(block, 0, width, axis=dim), axis, backward)
-        block = jnp.concatenate([low, block, high], axis=dim)
-    return block
-
-
-def in_one_piece(arrays, axis, dim, along):
-    widths = [math.prod(a.shape[along:]) for a in arrays]
-    both = jnp.concatenate(
-        [a.reshape(*a.shape[:along], w) for a, w in zip(arrays, widths)], axis=along
-    )
-    filled = lax.all_gather(both, axis, axis=dim, tiled=True)
-    parts = jnp.split(filled, [sum(widths[:k]) for k in range(1, len(widths))], axis=along)
-    return tuple(
-        (b.reshape(*filled.shape[:along], *a.shape[along:]) for a, b in zip(arrays, parts))
-    )
-
-
-def centred_conv(padded, weights, series_count):
-    summed = jnp.zeros((series_count, padded.shape[1]), jnp.float32)
-    for offset in range(weights.shape[0]):
-        summed = summed + weights[offset].astype(jnp.float32) * padded[
-            offset : offset + series_count
-        ].astype(jnp.float32)
-    return jax.nn.silu(summed)
-
-
-def local_sweep(inputs, entry_state, readout_state, log_fade_factor, softplus_increment):
-    seq_len = inputs.shape[0]
-    blocks = seq_len // BLOCK
-    heads_here = log_fade_factor.shape[0]
-    groups_here = entry_state.shape[1] // STATE
-    per_group = heads_here // groups_here
-    values = inputs.reshape(blocks, BLOCK, groups_here, per_group, HEAD_DIM)
-    b_blocks = entry_state.reshape(blocks, BLOCK, groups_here, STATE)
-    c_blocks = readout_state.reshape(blocks, BLOCK, groups_here, STATE)
-    decay_blocks = log_fade_factor.reshape(groups_here, per_group, blocks, BLOCK)
-    step_blocks = softplus_increment.reshape(groups_here, per_group, blocks, BLOCK)
-    cumulative = jnp.cumsum(decay_blocks, axis=-1)
-    group_inner = jnp.einsum("bign,bjgn->gbij", c_blocks, b_blocks)
-    spread = cumulative[..., :, None] - cumulative[..., None, :]
-    lower_tri = jnp.arange(BLOCK)[:, None] >= jnp.arange(BLOCK)[None, :]
-    mixing = (
-        jnp.exp(jnp.where(lower_tri, spread, -jnp.inf))
-        * step_blocks[..., None, :]
-        * group_inner[:, None]
-    )
-    within = jnp.einsum("gkbij,bjgkp->bigkp", mixing, values)
-    to_end = jnp.exp(cumulative[..., -1:] - cumulative) * step_blocks
-    block_states = jnp.einsum("gkbj,bjgkp,bjgn->bgkpn", to_end, values, b_blocks)
-    block_decay = cumulative[..., -1]
-
-    def advance(carried, pieces):
-        state_piece, decay_piece = pieces
-        return (carried * jnp.exp(decay_piece)[..., None, None] + state_piece, carried)
-
-    zero_state = jnp.zeros((groups_here, per_group, HEAD_DIM, STATE), jnp.float32)
-    final_state, entering = lax.scan(
-        advance, zero_state, (block_states, jnp.moveaxis(block_decay, -1, 0))
-    )
-    before = jnp.cumsum(block_decay, axis=-1) - block_decay
-    return (
-        (within, entering, cumulative, before, c_blocks),
-        (jnp.sum(block_decay, axis=-1), final_state),
-    )
-
-
-def finish_sweep(parts, carried):
-    within, entering, cumulative, before, c_blocks = parts
-    entering = entering + carried[None] * jnp.exp(jnp.moveaxis(before, -1, 0))[..., None, None]
-    readout = jnp.einsum("bign,bgkpn->bigkp", c_blocks, entering)
-    readout = readout * jnp.exp(jnp.transpose(cumulative, (2, 3, 0, 1)))[..., None]
-    combined = within + readout
-    return combined.reshape(combined.shape[0] * combined.shape[1], -1)
-
-
-def blend_parts_list(
-    channel_feed_bordered,
-    write_coefficient_bordered,
-    emission_coefficient_bordered,
-    channel_feed_taps,
-    write_coefficient_taps,
-    emission_coefficient_taps,
-    raw_increments,
-    channel_log_fade_speed,
-    extra_log_fade,
-    series_count,
-):
-    inputs = centred_conv(channel_feed_bordered, channel_feed_taps, series_count)
-    entry_state = centred_conv(write_coefficient_bordered, write_coefficient_taps, series_count)
-    readout_state = centred_conv(
-        emission_coefficient_bordered, emission_coefficient_taps, series_count
-    )
-    softplus_increment = jax.nn.softplus(raw_increments.astype(jnp.float32))
-    log_fade_factor = (
-        -softplus_increment * jnp.exp(channel_log_fade_speed)[..., None] + extra_log_fade
-    )
-    onward_pass = local_sweep(
-        inputs, entry_state, readout_state, log_fade_factor[0], softplus_increment[0]
-    )
-    backward_pass = local_sweep(
-        jnp.flip(inputs, 0),
-        jnp.flip(entry_state, 0),
-        jnp.flip(readout_state, 0),
-        jnp.flip(log_fade_factor[1], -1),
-        jnp.flip(softplus_increment[1], -1),
-    )
-    return (onward_pass, backward_pass)
-
-
-def gated_norm(mixed_sum, result_switch_mapped, cluster_scaling_factor):
-    gated = mixed_sum * jax.nn.silu(result_switch_mapped.astype(jnp.float32))
-    grouped = gated.reshape(gated.shape[0], -1, INNER // GROUPS)
-    normalized = grouped * lax.rsqrt(jnp.mean(grouped * grouped, axis=-1, keepdims=True) + EPSILON)
-    return (normalized.reshape(gated.shape) * cluster_scaling_factor).astype(jnp.bfloat16)
-
-
-def fold_summaries(gathered, position):
-    fwd_totals, fwd_finals, bwd_totals, bwd_finals = gathered
-    device_order = jnp.arange(fwd_totals.shape[0], dtype=jnp.int32)[:, None, None]
-    earlier = device_order < position
-    later_side = device_order > position
-    fwd_running = jnp.cumsum(fwd_totals, axis=0)
-    fwd_reach = jnp.sum(jnp.where(earlier, fwd_totals, 0.0), axis=0)
-    fwd_weight = jnp.exp(jnp.where(earlier, fwd_reach - fwd_running, -jnp.inf))
-    bwd_running = jnp.cumsum(bwd_totals, axis=0)
-    bwd_reach = jnp.sum(jnp.where(device_order <= position, bwd_totals, 0.0), axis=0)
-    bwd_weight = jnp.exp(jnp.where(later_side, bwd_running - bwd_totals - bwd_reach, -jnp.inf))
-    carried_fwd = jnp.einsum("jgk,jgkpn->gkpn", fwd_weight, fwd_finals)
-    carried_bwd = jnp.einsum("jgk,jgkpn->gkpn", bwd_weight, bwd_finals)
-    return (carried_fwd, carried_bwd)
-
 
 MESH = pl.DeviceIdType.MESH
 F32 = jnp.float32
@@ -575,6 +427,335 @@
     )
 
 
+def over_lanes(columns, direction):
+    rows = columns.shape[0]
+    low = lax.broadcasted_iota(jnp.int32, (rows, 128), 1) < HEAD_DIM
+    pairs = []
+    for pair in range(2):
+        at = 4 * direction + 2 * pair
+        pairs.append(jnp.where(low, columns[:, at : at + 1], columns[:, at + 1 : at + 2]))
+    return jnp.concatenate(pairs, axis=1)
+
+
+def mixer_kernel(
+    feed_ref,
+    write_ref,
+    read_ref,
+    feed_taps,
+    write_taps,
+    read_taps,
+    raw_ref,
+    fade_ref,
+    extra_ref,
+    switch_ref,
+    gain_ref,
+    out_ref,
+    rim,
+    padded,
+    feed,
+    write,
+    read,
+    decay_s,
+    step_s,
+    columns,
+    states,
+    mixed,
+    ends_out,
+    ends_in,
+    totals_in,
+    carry_out,
+    carry_in,
+    totals_out,
+    rim_send,
+    rim_recv,
+    end_send,
+    end_recv,
+    total_send,
+    total_recv,
+    carry_send,
+    carry_recv,
+):
+    s, t = lax.axis_index("sp"), lax.axis_index("tp")
+    after_me, before_me = lax.rem(s + 1, NS), lax.rem(s + NS - 1, NS)
+    greet((), True)
+
+    spans = ((feed_ref, 0, 256), (write_ref, 256, 384), (read_ref, 384, 512))
+    rims = []
+    for k, (source, start, stop) in enumerate(spans):
+        rims.append(
+            remote(
+                source.at[pl.ds(504, 8)],
+                rim.at[0, :, start:stop],
+                rim_send.at[k],
+                rim_recv.at[k],
+                after_me,
+                t,
+            )
+        )
+        rims.append(
+            remote(
+                source.at[pl.ds(0, 8)],
+                rim.at[1, :, start:stop],
+                rim_send.at[3 + k],
+                rim_recv.at[3 + k],
+                before_me,
+                t,
+            )
+        )
+    for copy in rims:
+        copy.start()
+    for source, start, stop in spans:
+        padded[8:520, start:stop] = source[...].astype(F32)
+
+    for direction in range(2):
+        raw = raw_ref[direction].astype(F32)
+        step = jnp.maximum(raw, 0.0) + jnp.log1p(jnp.exp(-jnp.abs(raw)))
+        head = lax.broadcasted_iota(jnp.int32, (4, 512), 0)
+        fade = jnp.zeros((4, 512), F32)
+        for h in range(4):
+            fade = jnp.where(head == h, fade_ref[direction, h], fade)
+        step_s[4 * direction : 4 * direction + 4, :] = step
+        decay_s[4 * direction : 4 * direction + 4, :] = extra_ref[direction] - step * jnp.exp(fade)
+
+    row = lax.broadcasted_iota(jnp.int32, (BLOCK, BLOCK), 0)
+    col = lax.broadcasted_iota(jnp.int32, (BLOCK, BLOCK), 1)
+    upto = jnp.where(row <= col, 1.0, 0.0)
+    onward = jnp.where(row >= col, 1.0, 0.0)
+    forward_rows = lax.broadcasted_iota(jnp.int32, (8, BLOCK), 0) < 4
+    forward_lanes = lax.broadcasted_iota(jnp.int32, (1, 8), 1) < 4
+    totals = []
+    for b in range(4):
+        span = slice(b * BLOCK, (b + 1) * BLOCK)
+        piece = decay_s[:, span]
+        run = jnp.where(
+            forward_rows,
+            jnp.dot(piece, upto, precision=HIGH, preferred_element_type=F32),
+            jnp.dot(piece, onward, precision=HIGH, preferred_element_type=F32),
+        )
+        decay_s[:, span] = run
+        run_columns = run.T
+        total = jnp.where(
+            forward_lanes, run_columns[BLOCK - 1 : BLOCK, :], run_columns[0:1, :]
+        )
+        totals.append(total)
+        columns[0, b] = run_columns
+        columns[1, b] = jnp.exp(total - run_columns) * step_s[:, span].T
+
+    for copy in rims:
+        copy.wait_recv()
+    padded[0:8, :] = jnp.where(s > 0, rim[0].astype(F32), 0.0)
+    padded[520:528, :] = jnp.where(s < NS - 1, rim[1].astype(F32), 0.0)
+
+    for b in range(4):
+        span = slice(b * BLOCK, (b + 1) * BLOCK)
+        for taps, start, stop in (
+            (feed_taps, 0, 256),
+            (write_taps, 256, 384),
+            (read_taps, 384, 512),
+        ):
+            summed = None
+            for offset in range(CONV_W):
+                term = taps[offset : offset + 1, :].astype(F32) * padded[
+                    b * BLOCK + 6 + offset : b * BLOCK + 6 + offset + BLOCK, start:stop
+                ]
+                summed = term if summed is None else summed + term
+            summed = summed * jax.nn.sigmoid(summed)
+            if start == 0:
+                feed[span, :] = summed
+            elif start == 256:
+                write[span, :] = summed
+            else:
+                read[span, :] = summed.astype(BF16)
+
+    for b in range(4):
+        span = slice(b * BLOCK, (b + 1) * BLOCK)
+        ends = columns[1, b]
+        x = feed[span, :]
+        scaled = jnp.concatenate([x * over_lanes(ends, 0), x * over_lanes(ends, 1)], axis=1)
+        states[b] = matmul(write[span, :].T.astype(BF16), scaled.astype(BF16))
+    final = []
+    for direction in range(2):
+        lanes = slice(256 * direction, 256 * direction + 256)
+        entering = jnp.zeros((STATE, 256), F32)
+        for b in (range(4), range(3, -1, -1))[direction]:
+            own = states[b, :, lanes]
+            states[b, :, lanes] = entering
+            entering = entering * jnp.exp(over_lanes(totals[b], direction)) + own
+        final.append(entering.reshape(NS, 8, 256))
+    ends_out[...] = jnp.concatenate(final, axis=1).astype(BF16)
+    whole = totals[0] + totals[1] + totals[2] + totals[3]
+    totals_out[...] = jnp.zeros((8, 128), F32)
+    for direction in range(2):
+        flat = over_lanes(whole, direction)
+        for pair in range(2):
+            at = 2 * direction + pair
+            totals_out[at : at + 1, :] = flat[:, 128 * pair : 128 * pair + 128]
+
+    def send_ends(k, carry):
+        peer = lax.rem(s + k, NS)
+        remote(ends_out.at[peer], ends_in.at[s], end_send.at[k], end_recv.at[k], peer, t).start()
+        remote(totals_out, totals_in.at[s], total_send.at[k], total_recv.at[k], peer, t).start()
+        return carry
+
+    lax.fori_loop(1, NS, send_ends, 0)
+    ends_in[s] = ends_out[s]
+    totals_in[s] = totals_out[...]
+
+    def within(b):
+        span = slice(b * BLOCK, (b + 1) * BLOCK)
+        inner = lax.dot_general(
+            read[span, :],
+            write[span, :].astype(BF16),
+            (((1,), (1,)), ((), ())),
+            preferred_element_type=F32,
+        )
+        run, step, run_columns = decay_s[:, span], step_s[:, span], columns[0, b]
+        low = col < HEAD_DIM
+        for pair in range(2):
+            x = feed[span, 128 * pair : 128 * pair + 128].astype(BF16)
+            parts = []
+            for h in (2 * pair, 2 * pair + 1):
+                k = 4 + h
+                onto = jnp.exp(
+                    jnp.where(row >= col, run_columns[:, h : h + 1] - run[h : h + 1, :], -jnp.inf)
+                ) * step[h : h + 1, :]
+                back = jnp.exp(
+                    jnp.where(row <= col, run_columns[:, k : k + 1] - run[k : k + 1, :], -jnp.inf)
+                ) * step[k : k + 1, :]
+                parts.append(matmul(((onto + back) * inner).astype(BF16), x))
+            mixed[span, 128 * pair : 128 * pair + 128] = jnp.where(low, parts[0], parts[1])
+
+    within(0)
+    within(1)
+
+    def await_ends(k, carry):
+        remote(ends_out.at[s], ends_in.at[s], end_send.at[k], end_recv.at[k], s, t).wait_recv()
+        remote(totals_out, totals_in.at[s], total_send.at[k], total_recv.at[k], s, t).wait_recv()
+        return carry
+
+    lax.fori_loop(1, NS, await_ends, 0)
+    def total_of(p, direction):
+        pairs = [totals_in[p, 2 * direction + k : 2 * direction + k + 1, :] for k in range(2)]
+        return jnp.exp(jnp.concatenate(pairs, axis=1))
+
+    running = jnp.zeros((8, 256), F32)
+    for p in range(NS):
+        carry_out[p, 0:8, :] = running.astype(BF16)
+        running = running * total_of(p, 0) + ends_in[p, 0:8, :].astype(F32)
+    running = jnp.zeros((8, 256), F32)
+    for p in range(NS - 1, -1, -1):
+        carry_out[p, 8:16, :] = running.astype(BF16)
+        running = running * total_of(p, 1) + ends_in[p, 8:16, :].astype(F32)
+
+    def send_carry(k, carry):
+        peer = lax.rem(s + k, NS)
+        remote(
+            carry_out.at[peer], carry_in.at[s], carry_send.at[k], carry_recv.at[k], peer, t
+        ).start()
+        return carry
+
+    lax.fori_loop(1, NS, send_carry, 0)
+    carry_in[s] = carry_out[s]
+    within(2)
+    within(3)
+
+    def await_carry(k, carry):
+        remote(
+            carry_out.at[s], carry_in.at[s], carry_send.at[k], carry_recv.at[k], s, t
+        ).wait_recv()
+        return carry
+
+    lax.fori_loop(1, NS, await_carry, 0)
+    carried = carry_in[...].astype(F32)
+    carried = (carried[:, 0:8, :].reshape(STATE, 256), carried[:, 8:16, :].reshape(STATE, 256))
+    ahead = (
+        jnp.zeros((1, 8), F32),
+        totals[0],
+        totals[0] + totals[1],
+        totals[0] + totals[1] + totals[2],
+    )
+    behind = (
+        totals[1] + totals[2] + totals[3],
+        totals[2] + totals[3],
+        totals[3],
+        jnp.zeros((1, 8), F32),
+    )
+    for b in range(4):
+        span = slice(b * BLOCK, (b + 1) * BLOCK)
+        entering = jnp.concatenate(
+            [
+                carried[0] * jnp.exp(over_lanes(ahead[b], 0)),
+                carried[1] * jnp.exp(over_lanes(behind[b], 1)),
+            ],
+            axis=1,
+        )
+        readout = matmul(read[span, :], (states[b] + entering).astype(BF16))
+        reach = jnp.exp(columns[0, b])
+        total = (
+            mixed[span, :]
+            + readout[:, 0:256] * over_lanes(reach, 0)
+            + readout[:, 256:512] * over_lanes(reach, 1)
+        )
+        switch = switch_ref[span, :].astype(F32)
+        gated = total * (switch * jax.nn.sigmoid(switch))
+        scale = lax.rsqrt(jnp.mean(gated * gated, axis=-1, keepdims=True) + EPSILON)
+        out_ref[span, :] = (gated * scale * gain_ref[...]).astype(BF16)
+
+    for copy in rims:
+        copy.wait_send()
+
+    def end_sends(k, carry):
+        remote(ends_out.at[s], ends_in.at[s], end_send.at[k], end_recv.at[k], s, t).wait_send()
+        remote(totals_out, totals_in.at[s], total_send.at[k], total_recv.at[k], s, t).wait_send()
+        remote(
+            carry_out.at[s], carry_in.at[s], carry_send.at[k], carry_recv.at[k], s, t
+        ).wait_send()
+        return carry
+
+    lax.fori_loop(1, NS, end_sends, 0)
+
+
+def mix(feed, write, read, taps, raw, fade, extra, switch, gain):
+    vmem = pl.BlockSpec(memory_space=pltpu.VMEM)
+    smem = pl.BlockSpec(memory_space=pltpu.SMEM)
+    dma = pltpu.SemaphoreType.DMA
+    return pl.pallas_call(
+        mixer_kernel,
+        out_shape=jax.ShapeDtypeStruct((512, 256), BF16),
+        in_specs=[vmem] * 7 + [smem] + [vmem] * 3,
+        out_specs=vmem,
+        scratch_shapes=[
+            pltpu.VMEM((2, 8, 512), BF16),
+            pltpu.VMEM((528, 512), F32),
+            pltpu.VMEM((512, 256), F32),
+            pltpu.VMEM((512, 128), F32),
+            pltpu.VMEM((512, 128), BF16),
+            pltpu.VMEM((8, 512), F32),
+            pltpu.VMEM((8, 512), F32),
+            pltpu.VMEM((2, 4, 128, 8), F32),
+            pltpu.VMEM((4, 128, 512), F32),
+            pltpu.VMEM((512, 256), F32),
+            pltpu.VMEM((NS, 16, 256), BF16),
+            pltpu.VMEM((NS, 16, 256), BF16),
+            pltpu.VMEM((NS, 8, 128), F32),
+            pltpu.VMEM((NS, 16, 256), BF16),
+            pltpu.VMEM((NS, 16, 256), BF16),
+            pltpu.VMEM((8, 128), F32),
+            dma((6,)),
+            dma((6,)),
+            dma((NS,)),
+            dma((NS,)),
+            dma((NS,)),
+            dma((NS,)),
+            dma((NS,)),
+            dma((NS,)),
+        ],
+        compiler_params=pltpu.CompilerParams(
+            collective_id=1, has_side_effects=True, vmem_limit_bytes=40 * 1024 * 1024
+        ),
+    )(feed, write, read, *taps, raw, fade, extra, switch, gain.reshape(1, 256))
+
+
 def per_device(
     skip_stream_entry,
     result_switch_mapped,
@@ -596,56 +777,17 @@
     picked_specialists,
     router_affinities,
 ):
-    series_count = channel_feed_mapped.shape[0]
-    rim_width = CONV_W // 2
-    sources = (channel_feed_mapped, write_coefficient_mapped, emission_coefficient_mapped)
-    edges = jnp.concatenate(
-        [jnp.concatenate([source[:rim_width], source[-rim_width:]], 0) for source in sources], 1
-    )
-    rimmed = with_halo(edges, (("sp", 0),), rim_width)
-    padded_list = []
-    column_start = 0
-    for source in sources:
-        width_here = source.shape[1]
-        upper_rim = rimmed[:rim_width, column_start : column_start + width_here]
-        lower_rim = rimmed[-rim_width:, column_start : column_start + width_here]
-        padded_list.append(jnp.concatenate([upper_rim, source, lower_rim], 0))
-        column_start = column_start + width_here
-    onward_pass, backward_pass = blend_parts_list(
-        padded_list[0],
-        padded_list[1],
-        padded_list[2],
-        channel_feed_taps,
-        write_coefficient_taps,
-        emission_coefficient_taps,
+    mixed_rows = mix(
+        channel_feed_mapped,
+        write_coefficient_mapped,
+        emission_coefficient_mapped,
+        (channel_feed_taps, write_coefficient_taps, emission_coefficient_taps),
         raw_increments,
         channel_log_fade_speed,
         extra_log_fade,
-        series_count,
-    )
-    fwd_total, fwd_final = onward_pass[1]
-    bwd_total, bwd_final = backward_pass[1]
-    gathered = tuple(
-        (
-            part.astype(jnp.float32)
-            for part in in_one_piece(
-                (
-                    fwd_total[None].astype(jnp.bfloat16),
-                    fwd_final[None].astype(jnp.bfloat16),
-                    bwd_total[None].astype(jnp.bfloat16),
-                    bwd_final[None].astype(jnp.bfloat16),
-                ),
-                "sp",
-                0,
-                3,
-            )
-        )
-    )
-    carried_fwd, carried_bwd = fold_summaries(gathered, lax.axis_index("sp"))
-    mixed_sum = finish_sweep(onward_pass[0], carried_fwd) + jnp.flip(
-        finish_sweep(backward_pass[0], carried_bwd), 0
-    )
-    mixed_rows = gated_norm(mixed_sum, result_switch_mapped, cluster_scaling_factor)
+        result_switch_mapped,
+        cluster_scaling_factor,
+    )
     return finish_layer(
         mixed_rows,
         blend_result_matrix,

time: 217 us -> 150 us (0.69)
  waiting for transfers between devices: 47.8 us -> 0 us
  Pallas kernels: 112 us -> 136 us
  between operations: 14 us -> 0.04 us
  other arithmetic: 9.7 us -> 0 us
  local copies, waits for them, and re-layouts: 21.4 us -> 13.5 us
  matrix products: 6.32 us -> 0 us
  starting transfers between devices: 5.23 us -> 0 us
    all_gather x1 -> x0, waiting for transfers between devices: 47.7 us -> none  [in_one_piece(): filled = lax.all_gather(both, axis, axis=dim, tiled=True)]
    pallas_call x0 -> x1, Pallas kernels: none -> 22.1 us  [mix(): pl.pallas_call(mixer_kernel, out_shape=jax.ShapeDtypeStruct((512, 256), B...]
    unnamed x46 -> x27, local copies, waits for them, and re-layouts: 5.94 us -> 13.5 us
    dot_general x10 -> x0, matrix products: 6.32 us -> none  [the longest x2 1.83 us: local_sweep(): group_inner = jnp.einsum('bign,bjgn->gbij', c_blocks, b_blocks)]
    ppermute x2 -> x0, starting transfers between devices: 5.23 us -> none  [the longest x1 3.94 us: with_halo(): lax.ppermute(lax.slice_in_dim(block, block.shape[dim] - width, None, axis...]
    split x2 -> x0, local copies, waits for them, and re-layouts: 3.8 us -> none  [in_one_piece(): jnp.split(filled, [sum(widths[:k]) for k in range(1, len(widths))], axis=...]
    mul x9 -> x0, other arithmetic: 3.25 us -> none  [the longest x3 1.76 us: centred_conv(): weights[offset].astype(jnp.float32)]
    another operation x6 -> x0, other arithmetic: 2.85 us -> none  [the longest x2 2.42 us: local_sweep(): cumulative = jnp.cumsum(decay_blocks, axis=-1)]
  transfers between devices with their start and end apart: 3 -> 0, of which waited for: 1 -> 0; matrix products, arithmetic and copies ran while one was open for 6% -> 0% of each run, Pallas kernels for 0% -> 0%
where the time goes in v3:
time: 150 us; the launch traced here: 149 us
  Pallas kernels  136 us (91%)
  local copies, waits for them, and re-layouts  13.5 us (9%)
    pallas_call x1, Pallas kernels, finish_layer(): pl.pallas_call(moe_kernel, out_shape=jax.ShapeDtypeStruct((32, WIDTH), BF...  113 us
    pallas_call x1, Pallas kernels, mix(): pl.pallas_call(mixer_kernel, out_shape=jax.ShapeDtypeStruct((512, 256), B...  22.1 us
    unnamed x27, local copies, waits for them, and re-layouts  13.5 us

profile of v3, /device:TPU:1, one launch (start us, length us, event | category | flops | bytes accessed | tf_op | source)
XLA Modules:
  0.0 149.1 jit_solution(4758685913894224990)
XLA Ops:
  0.0 1.4 copy.20.picks_ref
  1.4 1.4 copy.21.affinity_ref
  2.7 0.0 copy-start.1
  2.7 0.9 copy-done.1
  3.7 0.0 copy-start.2
  3.7 0.9 copy-done.2
  4.6 0.0 copy-start.3
  4.6 0.9 copy-done.3
  5.5 0.0 copy-start.4
  5.5 0.9 copy-done.4
  6.4 0.0 copy-start.5
  6.4 0.7 copy-done.5
  7.1 0.0 copy-start.6
  7.1 0.7 copy-done.6
  7.8 0.0 copy-start.7
  7.8 0.7 copy-done.7
  8.5 0.0 copy-start.8
  8.5 0.7 copy-done.8
  9.2 0.0 copy-start.9
  9.2 0.7 copy-done.9
  9.9 0.0 copy-start.10
  9.9 0.7 copy-done.10
  10.6 0.0 copy-start.11
  10.6 0.7 copy-done.11
  11.3 22.1 %shard_map.181 = bf16[512,256]{1,0:T(8,128)(2,1)S(1)} custom-call(bf16[512,256]{1,0:T(8,128)(2,1)S(1)} %copy-done.1, bf16[512,128]{1,0:T(8,128)(2,1)S(1)} %copy-done.3, bf16[512,128]{1,0:T(8,128)(2,1)S(1)} %copy-done.4, bf16[5,256]{1,0:T(8,128)(2,1)S(1)} %copy-done.7, bf16[5,128]{1,0:T(8,128)(2,1)S(1)} %copy-done.8, bf16[5,128]{1,0:T(8,128)(2,1)S(1)} %copy-done.9, ...), custom_call_target="tpu_custom_call" | custom-call | tf_op jit(solution)/shard_map/pallas_call | solution.py:722
  33.4 0.0 copy-start
  33.4 0.7 copy-done
  34.1 113.5 %shard_map.182 = bf16[32,2048]{1,0:T(8,128)(2,1)} custom-call(bf16[8,2,32,256]{3,2,1,0:T(8,128)(2,1)} %bitcast.3, bf16[256,2048]{1,0:T(8,128)(2,1)} %blend_ref.1, bf16[32,2048]{1,0:T(8,128)(2,1)} %skip_ref.1, f32[1,2048]{1,0:T(1,128)} %bitcast.5, s32[32,2]{1,0:T(8,128)} %copy.20.picks_ref, f32[32,2]{1,0:T(8,128)} %copy.21.affinity_ref, ...), custom_call_target="tpu_custom_call" | custom-call | tf_op jit(solution)/shard_map/pallas_call | solution.py:373
  147.6 1.6 %copy.23 = bf16[32,2048]{1,0:T(8,128)(2,1)} copy(bf16[32,2048]{1,0:T(8,128)(2,1)} %shard_map.182) | data formatting | bytes 262144
Async XLA Ops:
  2.7 0.9 copy-start.1
  3.7 0.9 copy-start.2
  4.6 0.9 copy-start.3
  5.5 0.9 copy-start.4
  6.4 0.7 copy-start.5
  7.1 0.7 copy-start.6
  7.8 0.7 copy-start.7
  8.5 0.7 copy-start.8
  9.2 0.7 copy-start.9
  9.9 0.7 copy-start.10
  10.6 0.7 copy-start.11
  33.4 0.7 copy-start
